TPU v7x, 512 devices: a 4x2x32 block of a 4x8x32 slice. The times are simulated.
512 devices in a mesh: grp: 2 (over y), fs: 32 (over z), tp: 8 (over x, core).
Axes of the slice: x: 4, y: 2, z: 32, core: 2. Of those that a mesh axis runs over, the one named last changes fastest.
The devices are a block of a 4x8x32 slice.
Arguments:
- tokens: bfloat16 [8192, 2048], P(('grp', 'fs')), parts along dimension 0, may hold values from -6 to 6
- pre_attention_gain: float32 [2048], replicated, may hold values from 0.1 to 1.9
- query_weight: bfloat16 [2048, 512], P('fs', 'tp'), may hold values from -0.125 to 0.125
- key_weight: bfloat16 [2048, 512], P('fs', 'tp'), may hold values from -0.125 to 0.125
- value_weight: bfloat16 [2048, 1024], P('fs', 'tp'), may hold values from -0.125 to 0.125
- output_gate_weight: bfloat16 [2048, 1024], P('fs', 'tp'), may hold values from -0.125 to 0.125
- decay_weight: bfloat16 [2048, 512], P('fs', 'tp'), may hold values from -0.25 to 0.25
- decay_logit_bias: float32 [512], P('tp'), may hold values from -1 to 4
- extra_log_decay: float32 [8192, 512], P(('grp', 'fs'), 'tp'), parts along dimension 0, may hold values from -0.7 to 0
- head_norm_gain: float32 [1024], P('tp'), may hold values from 0.1 to 1.9
- attention_out_weight: bfloat16 [1024, 2048], P('tp', 'fs'), may hold values from -0.1875 to 0.1875
- post_attention_gain: float32 [2048], replicated, may hold values from 0.1 to 1.9
- pre_feedforward_gain: float32 [2048], replicated, may hold values from 0.1 to 1.9
- post_feedforward_gain: float32 [2048], replicated, may hold values from 0.1 to 1.9
- up_weight: bfloat16 [2048, 8192], P('fs', 'tp'), may hold values from -0.125 to 0.125
- down_weight: bfloat16 [8192, 2048], P('tp', 'fs'), may hold values from -0.0625 to 0.0625
Outputs:
- layer_out: bfloat16 [8192, 2048], P(('grp', 'fs')), parts along dimension 0
There are 2 independent parts, one for each index of `grp`. A program takes and returns all parts, laid end to end along the dimension named above; an argument that names none is the same for every part. Nothing has to cross between parts.
All inputs are finite; a program needn't handle non-finite values.
Results may differ from a plain program's by a relative error of at most 0.035.
Values may be sent and summed in bfloat16 or wider, within the bound.
No kernel may reach another device: no remote copies, remote signals or barrier semaphores. Data moves between devices by JAX's collectives and lax.ppermute only.
A program may use at most 64 MiB of HBM per device.

v0:
```python
import functools

import jax
import jax.numpy as jnp
from jax import lax
from jax.experimental import pallas as pl
from jax.experimental.pallas import tpu as pltpu
from jax.sharding import PartitionSpec as P


DK = 64
DV = 128
SUB = 8

EPS = 1e-06
GATE_NORM_SCALE = 16.0
WEIGHT_SCALE = 2.0**16
HIGH = lax.Precision.HIGHEST
F32 = jnp.float32
BF16 = jnp.bfloat16


def root_norm(rows, gain):
    return rows * lax.rsqrt(jnp.mean(rows * rows, axis=-1, keepdims=True) + EPS) * gain


def attend_body(acc_ref, bias_ref, extra_ref, gain_ref, out_ref):
    length = acc_ref.shape[0]
    subs = length // SUB
    rounded = lambda lo, hi: acc_ref[:, lo:hi].astype(BF16).astype(F32)
    v = rounded(0, DV)
    g = rounded(DV, 2 * DV)
    q = rounded(2 * DV, 2 * DV + DK) * DK ** (-0.5)
    k = rounded(2 * DV + DK, 2 * DV + 2 * DK)
    pre = acc_ref[:, 2 * DV + 2 * DK : 2 * DV + 3 * DK] + bias_ref[...]
    log_sig = jnp.minimum(pre, 0.0) - jnp.log1p(jnp.exp(-jnp.abs(pre)))
    log_decay = log_sig / GATE_NORM_SCALE + extra_ref[...].T
    row = lax.broadcasted_iota(jnp.int32, (length, length), 0)
    col = lax.broadcasted_iota(jnp.int32, (length, length), 1)
    dot = functools.partial(lax.dot_general, precision=HIGH, preferred_element_type=F32)
    nn, nt = (((1,), (0,)), ((), ())), (((1,), (1,)), ((), ()))
    cum = dot((row >= col).astype(F32), log_decay, nn)
    cum3, q3, k3 = (a.reshape(subs, SUB, DK) for a in (cum, q, k))
    inside = []
    for j in range(SUB):
        gap = jnp.minimum(cum3 - cum3[:, j : j + 1, :], 0.0)
        inside.append(jnp.sum(q3 * k3[:, j : j + 1, :] * jnp.exp(gap), axis=-1, keepdims=True))
    near = jnp.zeros((length, length), F32)
    for j in range(SUB):
        near = jnp.where(lax.rem(col, SUB) == j, inside[j].reshape(length, 1), near)
    same = (row // SUB == col // SUB) & (row >= col)
    far = [jnp.zeros((SUB, length), F32)]
    for i in range(1, subs):
        at = i * SUB
        mark = cum[at - 1 : at, :]
        left = q[at : at + SUB, :] * jnp.exp(jnp.minimum(cum[at : at + SUB, :] - mark, 0.0))
        right = k * jnp.exp(jnp.minimum(mark - cum, 0.0))
        far.append(dot(left, right, nt))
    scores = jnp.where(same, near, jnp.where(row // SUB > col // SUB, jnp.concatenate(far, 0), 0.0))
    attended = dot(scores, v, nn)
    scaled = attended * lax.rsqrt(jnp.mean(attended * attended, axis=-1, keepdims=True) + EPS)
    out_ref[...] = (scaled * gain_ref[...] * (g / (1.0 + jnp.exp(-g)))).astype(out_ref.dtype)


def attend(acc, bias, extra, gain):
    length = acc.shape[0]
    return pl.pallas_call(
        attend_body,
        out_shape=jax.ShapeDtypeStruct((length, DV), BF16),
        compiler_params=pltpu.CompilerParams(vmem_limit_bytes=16 * 2**20),
        cost_estimate=pl.CostEstimate(flops=40_000_000, bytes_accessed=500_000, transcendentals=400_000),
        name="attend",
    )(acc, bias, extra, gain)


def feed_body(halves, rows_ref, weight_ref, part_ref, out_ref, sum_ref, act_ref):
    step = pl.program_id(0)

    @pl.when(step < halves)
    def _():
        product = jnp.dot(rows_ref[...], weight_ref[...], preferred_element_type=F32)

        @pl.when(step == 0)
        def _():
            sum_ref[...] = product

        @pl.when(step > 0)
        def _():
            sum_ref[...] += product

        @pl.when(step == halves - 1)
        def _():
            act_ref[...] = jnp.square(jnp.maximum(sum_ref[...], 0.0)).astype(BF16)

    @pl.when(step >= halves)
    def _():
        product = lax.dot_general(
            act_ref[...], weight_ref[...], (((1,), (1,)), ((), ())), preferred_element_type=F32
        )
        out_ref[...] = (product + part_ref[...]).astype(out_ref.dtype)


def feed(rows, both, part):
    length, width = rows.shape
    units = both.shape[1] // 2
    halves = 2
    block = width // halves
    later = lambda s: (0, jnp.maximum(s - halves, 0))
    return pl.pallas_call(
        functools.partial(feed_body, halves),
        grid=(2 * halves,),
        in_specs=[
            pl.BlockSpec((length, block), lambda s: (0, jnp.minimum(s, halves - 1))),
            pl.BlockSpec((block, units), lambda s: (lax.rem(s, halves), s // halves)),
            pl.BlockSpec((length, block), later),
        ],
        out_specs=pl.BlockSpec((length, block), later),
        out_shape=jax.ShapeDtypeStruct((length, width), BF16),
        scratch_shapes=[pltpu.VMEM((length, units), F32), pltpu.VMEM((length, units), BF16)],
        compiler_params=pltpu.CompilerParams(
            dimension_semantics=("arbitrary",), vmem_limit_bytes=48 * 2**20
        ),
        cost_estimate=pl.CostEstimate(
            flops=4 * length * width * units, bytes_accessed=4 * width * units, transcendentals=0
        ),
        name="feed",
    )(rows, both, part)


def pack_body(first, up_ref, down_ref, out_ref, held, arrived, left):
    width = up_ref.shape[1] - first
    brought = []
    for i, source in enumerate((up_ref, down_ref)):
        copy = pltpu.make_async_copy(source.at[:, pl.ds(first, width)], held.at[i], arrived.at[i])
        copy.start()
        brought.append(copy)
    sent = []
    for i, copy in enumerate(brought):
        copy.wait()
        out = pltpu.make_async_copy(held.at[i], out_ref.at[:, pl.ds(i * width, width)], left.at[i])
        out.start()
        sent.append(out)
    for out in sent:
        out.wait()


def pack(up, down, first):
    depth, width = up.shape[0], up.shape[1] - first
    return pl.pallas_call(
        functools.partial(pack_body, first),
        in_specs=[pl.BlockSpec(memory_space=pltpu.HBM)] * 2,
        out_specs=pl.BlockSpec(memory_space=pltpu.HBM),
        out_shape=jax.ShapeDtypeStruct((depth, 2 * width), up.dtype),
        scratch_shapes=[
            pltpu.VMEM((2, depth, width), up.dtype),
            pltpu.SemaphoreType.DMA((2,)),
            pltpu.SemaphoreType.DMA((2,)),
        ],
        compiler_params=pltpu.CompilerParams(vmem_limit_bytes=62 * 2**20),
        name="pack",
    )(up, down)


def share_of_sum(part, axis):
    peers = lax.axis_size(axis)
    blocks = part.reshape(peers, part.shape[0] // peers, part.shape[1])
    arrived = lax.all_to_all(blocks, axis, split_axis=0, concat_axis=0, tiled=True)
    return arrived.astype(F32).sum(axis=0)


def local(
    tokens,
    pre_attention_gain,
    query_weight,
    key_weight,
    value_weight,
    output_gate_weight,
    decay_weight,
    decay_logit_bias,
    extra_log_decay,
    head_norm_gain,
    attention_out_weight,
    post_attention_gain,
    pre_feedforward_gain,
    post_feedforward_gain,
    up_weight,
    down_weight,
):
    apart = up_weight.shape[1] // 8
    down_rows = down_weight.T
    both = lax.all_gather(pack(up_weight, down_rows, apart), "fs", axis=0, tiled=True)
    groups = lax.axis_size("grp")
    side = lax.rem(lax.axis_index("grp"), 2)
    first = side == 0
    projections = jnp.concatenate(
        [value_weight, output_gate_weight, query_weight, key_weight, decay_weight], 1
    )
    parts = (up_weight[:, :apart], down_rows[:, :apart], projections, attention_out_weight.T)
    sizes = [p.shape[1] // 2 for p in parts]
    halves = [p[:, h * n : (h + 1) * n] for h in range(2) for p, n in zip(parts, sizes)]
    half = lax.dynamic_slice_in_dim(
        jnp.concatenate(halves, 1), side * sum(sizes), sum(sizes), 1
    )
    sent = (half.astype(F32) * WEIGHT_SCALE).astype(jnp.float16)
    swap = lambda w: lax.ppermute(w, "grp", [(i, i ^ 1) for i in range(groups)])
    far_tokens = swap(tokens)
    held = lax.all_gather(sent, "fs", axis=0, tiled=True)
    far_tokens, held = lax.optimization_barrier((far_tokens, held))
    unscaled = lambda w, lo, hi: (w[:, lo:hi].astype(F32) * (1.0 / WEIGHT_SCALE)).astype(BF16)
    normed = lambda rows: root_norm(rows.astype(F32), pre_attention_gain).astype(BF16)
    edges = [sum(sizes[:i]) for i in range(5)]
    near = unscaled(held, edges[3], edges[4])
    far = swap(near)
    sent_home = jnp.dot(
        normed(far_tokens), unscaled(held, edges[2], edges[3]), preferred_element_type=F32
    )
    acc_far = swap(sent_home)
    tokens, held, sent_home = lax.optimization_barrier((tokens, held, sent_home))
    acc_near = jnp.dot(
        normed(tokens), unscaled(held, edges[2], edges[3]), preferred_element_type=F32
    )
    acc = jnp.concatenate(
        [jnp.where(first, acc_near, acc_far), jnp.where(first, acc_far, acc_near)], 1
    )
    headout = attend(acc, decay_logit_bias[None], extra_log_decay.T, head_norm_gain[None])

    low, high = headout[:, : sizes[3]], headout[:, sizes[3] :]
    mix_part = sum(
        lax.dot_general(h, w, (((1,), (1,)), ((), ())), preferred_element_type=F32)
        for h, w in ((jnp.where(first, low, high), near), (jnp.where(first, high, low), far))
    )
    mix_part, held = lax.optimization_barrier((mix_part.astype(BF16), held))
    mixed = share_of_sum(mix_part, "tp")
    apart_near = unscaled(held, 0, edges[2])
    apart_far = swap(apart_near)
    up_apart, down_apart = (
        jnp.concatenate([w[:, lo:hi] for w in (apart_near, apart_far)], 1)
        for lo, hi in zip(edges[:2], edges[1:3])
    )
    share = mixed.shape[0]
    own_tokens = lax.dynamic_slice_in_dim(tokens, lax.axis_index("tp") * share, share, 0)
    stream = own_tokens.astype(F32) + root_norm(mixed, post_attention_gain)
    normed_mid = root_norm(stream, pre_feedforward_gain).astype(BF16)
    rows = lax.all_gather(normed_mid, "tp", axis=0, tiled=True)
    act = jnp.square(jax.nn.relu(jnp.dot(rows, up_apart, preferred_element_type=F32))).astype(BF16)
    part = lax.dot_general(act, down_apart, (((1,), (1,)), ((), ())), preferred_element_type=F32)
    feed_share = share_of_sum(feed(rows, both, part), "tp")
    out_share = (stream + root_norm(feed_share, post_feedforward_gain)).astype(BF16)
    return lax.all_gather(out_share, "tp", axis=0, tiled=True)


def solution(mesh):
    return jax.shard_map(
        local,
        mesh=mesh,
        in_specs=(
            P(("grp", "fs"), None),
            P(),
            P("fs", "tp"),
            P("fs", "tp"),
            P("fs", "tp"),
            P("fs", "tp"),
            P("fs", "tp"),
            P("tp"),
            P(("grp", "fs"), "tp"),
            P("tp"),
            P("tp", "fs"),
            P(),
            P(),
            P(),
            P("fs", "tp"),
            P("tp", "fs"),
        ),
        out_specs=P(("grp", "fs"), None),
        check_vma=False,
    )
```

profile of v0, /device:TPU:33, one launch (start us, length us, event | category | flops | bytes accessed | tf_op | source)
XLA Modules:
  0.0 237.7 jit_solution(12423349692924406269)
XLA Ops:
  6.6 1.7 pack.1
  8.3 4.6 %collective-permute-start = (bf16[128,2048]{1,0:T(8,128)(2,1)}, bf16[128,2048]{1,0:T(8,128)(2,1)S(1)}, u32[]{:S(2)}, u32[]{:S(2)}) collective-permute-start(bf16[128,2048]{1,0:T(8,128)(2,1)} %param.16), channel_id=1, source_target_pairs={{0,256},{256,0},{1,257},{257,1},{2,258},{258,2},{3,259},{259,3},{4... | collective-permute-start | bytes 1572872 | tf_op jit(solution)/shard_map/ppermute | solution.py:205
  12.9 0.9 pad_maximum_fusion.1
  13.8 0.9 fusion.50
  14.7 0.9 fusion.48
  15.6 0.1 concatenate.21
  15.8 116.3 %all-gather.4 = f16[2048,416]{1,0:T(8,128)(2,1)S(1)} all-gather(f16[64,416]{1,0:T(8,128)(2,1)S(1)} %multiply_convert_fusion.7), channel_id=1, replica_groups=mesh['grp'=2,'fs'=32,'tp'=8] {'fs'}, dimensions={0}, use_global_device_ids=true | all-gather | bytes 1757184 | tf_op jit(solution)/shard_map/all_gather | solution.py:207
  132.1 0.2 fusion.4
  132.3 0.6 fusion.10
  133.0 2.3 collective-permute-start.1
  135.3 0.3 multiply_convert_fusion.5
  135.7 3.1 %collective-permute-start.2 = (bf16[2048,64]{1,0:T(8,128)(2,1)S(1)}, bf16[2048,64]{1,0:T(8,128)(2,1)S(1)}, u32[]{:S(2)}, u32[]{:S(2)}) collective-permute-start(bf16[2048,64]{1,0:T(8,128)(2,1)S(1)} %multiply_convert_fusion.5), channel_id=1, source_target_pairs={{0,256},{256,0},{1,257},{257,1},{2,258},{258,2},{3,259},{259,3},{4... | collective-permute-start | bytes 786440 | tf_op jit(solution)/shard_map/ppermute | solution.py:205
  138.9 0.2 fusion.7
  139.1 0.4 broadcast_select_fusion.1
  139.7 2.5 %attend.1 = bf16[128,128]{1,0:T(8,128)(2,1)S(1)} custom-call(f32[128,448]{1,0:T(8,128)S(1)} %pad_maximum_fusion.acc_ref, f32[1,64]{1,0:T(1,128)S(1)} %bitcast.11, f32[64,128]{1,0:T(8,128)S(1)} %bitcast.10, f32[1,128]{1,0:T(1,128)S(1)} %bitcast.12), custom_call_target="tpu_custom_call" | custom-call | flops 40000000 | bytes 500000 | tf_op jit(solution)/shard_map/attend/pallas_call | solution.py:67
  142.2 0.5 fusion.33
  142.8 3.4 %collective-permute-done.2 = bf16[2048,64]{1,0:T(8,128)(2,1)S(1)} collective-permute-done((bf16[2048,64]{1,0:T(8,128)(2,1)S(1)}, bf16[2048,64]{1,0:T(8,128)(2,1)S(1)}, u32[]{:S(2)}, u32[]{:S(2)}) %collective-permute-start.2) | collective-permute-done | bytes 262176 | tf_op jit(solution)/shard_map/ppermute | solution.py:205
  146.2 1.1 fusion
  147.5 3.0 %collective-permute-start.3 = (bf16[2048,128]{1,0:T(8,128)(2,1)S(1)}, bf16[2048,128]{1,0:T(8,128)(2,1)S(1)}, u32[]{:S(2)}, u32[]{:S(2)}) collective-permute-start(bf16[2048,128]{1,0:T(8,128)(2,1)S(1)} %multiply_convert_fusion.4), channel_id=1, source_target_pairs={{0,256},{256,0},{1,257},{257,1},{2,258},{258,2},{3,259},{259,3},{4... | collective-permute-start | bytes 1572872 | tf_op jit(solution)/shard_map/ppermute | solution.py:205
  150.5 19.9 %all-to-all-start = ((bf16[8,16,2048]{2,1,0:T(8,128)(2,1)}), bf16[8,16,2048]{2,1,0:T(8,128)(2,1)S(1)}, u32[]{:S(2)}, u32[]{:S(2)}) async-start(bf16[8,16,2048]{2,1,0:T(8,128)(2,1)} %bitcast.5), calls=%async_computation | async-start | bytes 1048576 | tf_op jit(solution)/shard_map/all_to_all | solution.py:167
  170.4 1.0 fusion.46
  171.5 8.4 %all-to-all-done = bf16[8,16,2048]{2,1,0:T(8,128)(2,1)S(1)} async-done(((bf16[8,16,2048]{2,1,0:T(8,128)(2,1)}), bf16[8,16,2048]{2,1,0:T(8,128)(2,1)S(1)}, u32[]{:S(2)}, u32[]{:S(2)}) %all-to-all-start) | async-done | bytes 524320 | tf_op jit(solution)/shard_map/all_to_all | solution.py:167
  180.0 0.1 multiply_reduce_fusion.2
  180.1 0.2 multiply_reduce_fusion.1
  180.4 14.0 %all_gather.13.rows_ref = bf16[128,2048]{1,0:T(8,128)(2,1)S(1)} all-gather(bf16[16,2048]{1,0:T(8,128)(2,1)S(1)} %multiply_convert_fusion.6), channel_id=1, replica_groups=mesh['grp'=2,'fs'=32,'tp'=8] {'tp'}, dimensions={0}, use_global_device_ids=true | all-gather | bytes 589824 | tf_op jit(solution)/shard_map/all_gather | solution.py:244
  194.4 1.1 fusion.47
  195.6 2.0 fusion.3.part_ref
  197.6 5.2 %feed.1 = bf16[128,2048]{1,0:T(8,128)(2,1)S(1)} custom-call(bf16[128,2048]{1,0:T(8,128)(2,1)S(1)} %all_gather.13.rows_ref, bf16[2048,1792]{1,0:T(8,128)(2,1)} %all-gather.3.cloned.1.call-done.weight_ref, f32[128,2048]{1,0:T(8,128)S(1)} %fusion.3.part_ref), custom_call_target="tpu_custom_call" | custom-call | flops 939524096 | bytes 7340032 | tf_op jit(solution)/shard_map/feed/pallas_call | solution.py:109
  202.7 12.0 %all_to_all.10 = bf16[8,16,2048]{2,1,0:T(8,128)(2,1)S(1)} all-to-all(bf16[8,16,2048]{2,1,0:T(8,128)(2,1)S(1)} %bitcast.9), channel_id=1, replica_groups=mesh['grp'=2,'fs'=32,'tp'=8] {'tp'}, dimensions={0} | all-to-all | bytes 1048576 | tf_op jit(solution)/shard_map/all_to_all | solution.py:167
  215.0 1.0 add_convert_fusion
  215.9 14.1 %all_gather.15 = bf16[128,2048]{1,0:T(8,128)(2,1)S(1)} all-gather(bf16[16,2048]{1,0:T(8,128)(2,1)S(1)} %add_convert_fusion), channel_id=1, replica_groups=mesh['grp'=2,'fs'=32,'tp'=8] {'tp'}, dimensions={0}, use_global_device_ids=true | all-gather | bytes 589824 | tf_op jit(solution)/shard_map/all_gather | solution.py:249
  230.0 0.8 copy.22
  (37 shorter events, 1.0 us)
Async XLA Ops:
  6.5 191.0 %all-gather.3.cloned.1.call-start = ((), (), s32[]{:S(2)}) async-start(), calls=%async_computation.2 | async-start | bytes 7569408 | tf_op jit(solution)/shard_map/all_gather | solution.py:191
  6.6 125.7 %copy-start.8 = (f32[2048]{0:T(1024)S(1)}, f32[2048]{0:T(1024)}, u32[]{:S(2)}) copy-start(f32[2048]{0:T(1024)} %param.17) | copy-start | bytes 24580
  8.3 123.8 %collective-permute-start = (bf16[128,2048]{1,0:T(8,128)(2,1)}, bf16[128,2048]{1,0:T(8,128)(2,1)S(1)}, u32[]{:S(2)}, u32[]{:S(2)}) collective-permute-start(bf16[128,2048]{1,0:T(8,128)(2,1)} %param.16), channel_id=1, source_target_pairs={{0,256},{256,0},{1,257},{257,1},{2,258},{258,2},{3,259},{259,3},{4... | collective-permute-start | bytes 1572872 | tf_op jit(solution)/shard_map/ppermute | solution.py:205
  132.3 6.6 %copy-start.4 = (bf16[128,2048]{1,0:T(8,128)(2,1)S(1)}, bf16[128,2048]{1,0:T(8,128)(2,1)}, u32[]{:S(2)}) copy-start(bf16[128,2048]{1,0:T(8,128)(2,1)} %param.16) | copy-start | bytes 1572868
  133.0 6.1 %collective-permute-start.1 = (f32[128,224]{1,0:T(8,128)S(1)}, f32[128,224]{1,0:T(8,128)S(1)}, u32[]{:S(2)}, u32[]{:S(2)}) collective-permute-start(f32[128,224]{1,0:T(8,128)S(1)} %copy.17), channel_id=1, source_target_pairs={{0,256},{256,0},{1,257},{257,1},{2,258},{258,2},{3,259},{259,3},{4... | collective-permute-start | bytes 344072 | tf_op jit(solution)/shard_map/ppermute | solution.py:205
  135.7 4.0 %copy-start = (f32[128,64]{0,1:T(8,128)S(1)}, f32[128,64]{0,1:T(8,128)}, u32[]{:S(2)}) copy-start(f32[128,64]{0,1:T(8,128)} %param.24) | copy-start | bytes 98308
  135.7 4.0 %copy-start.1 = (f32[64]{0:T(128)S(1)}, f32[64]{0:T(128)}, u32[]{:S(2)}) copy-start(f32[64]{0:T(128)} %param.23) | copy-start | bytes 772
  135.7 4.0 %copy-start.2 = (f32[128]{0:T(128)S(1)}, f32[128]{0:T(128)}, u32[]{:S(2)}) copy-start(f32[128]{0:T(128)} %param.25) | copy-start | bytes 1540
  135.7 10.5 %collective-permute-start.2 = (bf16[2048,64]{1,0:T(8,128)(2,1)S(1)}, bf16[2048,64]{1,0:T(8,128)(2,1)S(1)}, u32[]{:S(2)}, u32[]{:S(2)}) collective-permute-start(bf16[2048,64]{1,0:T(8,128)(2,1)S(1)} %multiply_convert_fusion.5), channel_id=1, source_target_pairs={{0,256},{256,0},{1,257},{257,1},{2,258},{258,2},{3,259},{259,3},{4... | collective-permute-start | bytes 786440 | tf_op jit(solution)/shard_map/ppermute | solution.py:205
  147.5 32.6 %copy-start.5 = (f32[2048]{0:T(1024)S(1)}, f32[2048]{0:T(1024)}, u32[]{:S(2)}) copy-start(f32[2048]{0:T(1024)} %param.27) | copy-start | bytes 24580
  147.5 32.8 %copy-start.6 = (f32[2048]{0:T(1024)S(1)}, f32[2048]{0:T(1024)}, u32[]{:S(2)}) copy-start(f32[2048]{0:T(1024)} %param.28) | copy-start | bytes 24580
  147.5 46.9 %collective-permute-start.3 = (bf16[2048,128]{1,0:T(8,128)(2,1)S(1)}, bf16[2048,128]{1,0:T(8,128)(2,1)S(1)}, u32[]{:S(2)}, u32[]{:S(2)}) collective-permute-start(bf16[2048,128]{1,0:T(8,128)(2,1)S(1)} %multiply_convert_fusion.4), channel_id=1, source_target_pairs={{0,256},{256,0},{1,257},{257,1},{2,258},{258,2},{3,259},{259,3},{4... | collective-permute-start | bytes 1572872 | tf_op jit(solution)/shard_map/ppermute | solution.py:205
  150.5 29.4 %all-to-all-start = ((bf16[8,16,2048]{2,1,0:T(8,128)(2,1)}), bf16[8,16,2048]{2,1,0:T(8,128)(2,1)S(1)}, u32[]{:S(2)}, u32[]{:S(2)}) async-start(bf16[8,16,2048]{2,1,0:T(8,128)(2,1)} %bitcast.5), calls=%async_computation | async-start | bytes 1048576 | tf_op jit(solution)/shard_map/all_to_all | solution.py:167
  194.4 1.1 copy-start.3
  197.5 17.4 %copy-start.7 = (f32[2048]{0:T(1024)S(1)}, f32[2048]{0:T(1024)}, u32[]{:S(2)}) copy-start(f32[2048]{0:T(1024)} %param.29) | copy-start | bytes 24580
Sparse Core Ops, SparseCore 0:
  9.4 165.9 all-gather.2
where the time goes:
time: 238 us
  blocking collectives  156 us (66%)
  starting transfers between devices  33 us (14%)
  between operations  13.7 us (6%)
  waiting for transfers between devices  12 us (5%)
  Pallas kernels  9.31 us (4%)
  local copies, waits for them, and re-layouts  4.97 us (2%)
  matrix products  4.67 us (2%)
  other arithmetic  3.64 us (2%)
    all_gather x1, blocking collectives, local(): held = lax.all_gather(sent, 'fs', axis=0, tiled=True)  116 us
    all_to_all x1, starting transfers between devices, share_of_sum(): lax.all_to_all(blocks, axis, split_axis=0, concat_axis=0, tiled=True)  19.9 us
    all_gather x1, blocking collectives, local(): return lax.all_gather(out_share, 'tp', axis=0, tiled=True)  14.1 us
    all_gather x1, blocking collectives, local(): rows = lax.all_gather(normed_mid, 'tp', axis=0, tiled=True)  14 us
    ppermute x4, starting transfers between devices, local(): swap = lambda w: lax.ppermute(w, 'grp', [(i, i ^ 1) for i in range(groups)])  13.1 us
    all_to_all x1, blocking collectives, share_of_sum(): lax.all_to_all(blocks, axis, split_axis=0, concat_axis=0, tiled=True)  12 us
    all_to_all x1, waiting for transfers between devices, share_of_sum(): lax.all_to_all(blocks, axis, split_axis=0, concat_axis=0, tiled=True)  8.43 us
    pallas_call x1, Pallas kernels, feed(): pl.pallas_call(functools.partial(feed_body, halves), grid=(2 * halves,),...  5.15 us
  transfers between devices with their start and end apart: 6, of which 3 were waited for; matrix products, arithmetic and copies ran while one was open for 5% of the time, Pallas kernels for 1%

commit v1 on v0

--- a/solution.py
+++ b/solution.py
@@ -4,6 +4,7 @@
 import jax.numpy as jnp
 from jax import lax
 from jax.experimental import pallas as pl
+from jax.experimental.layout import Layout, with_layout_constraint
 from jax.experimental.pallas import tpu as pltpu
 from jax.sharding import PartitionSpec as P
 
@@ -209,8 +210,6 @@
     unscaled = lambda w, lo, hi: (w[:, lo:hi].astype(F32) * (1.0 / WEIGHT_SCALE)).astype(BF16)
     normed = lambda rows: root_norm(rows.astype(F32), pre_attention_gain).astype(BF16)
     edges = [sum(sizes[:i]) for i in range(5)]
-    near = unscaled(held, edges[3], edges[4])
-    far = swap(near)
     sent_home = jnp.dot(
         normed(far_tokens), unscaled(held, edges[2], edges[3]), preferred_element_type=F32
     )
@@ -219,6 +218,9 @@
     acc_near = jnp.dot(
         normed(tokens), unscaled(held, edges[2], edges[3]), preferred_element_type=F32
     )
+    dense = lambda w: with_layout_constraint(w, Layout(major_to_minor=(0, 1)))
+    near = dense(dense(unscaled(held, edges[3], edges[4])).T)
+    far = dense(swap(near))
     acc = jnp.concatenate(
         [jnp.where(first, acc_near, acc_far), jnp.where(first, acc_far, acc_near)], 1
     )
@@ -226,7 +228,7 @@
 
     low, high = headout[:, : sizes[3]], headout[:, sizes[3] :]
     mix_part = sum(
-        lax.dot_general(h, w, (((1,), (1,)), ((), ())), preferred_element_type=F32)
+        jnp.dot(h, w, preferred_element_type=F32)
         for h, w in ((jnp.where(first, low, high), near), (jnp.where(first, high, low), far))
     )
     mix_part, held = lax.optimization_barrier((mix_part.astype(BF16), held))

time: 238 us -> 234 us (0.983)
  waiting for transfers between devices: 12 us -> 9.4 us
    ppermute x4, waiting for transfers between devices: 3.5 us -> 0.89 us  [local(): swap = lambda w: lax.ppermute(w, 'grp', [(i, i ^ 1) for i in range(groups)])]
where the time goes in v1:
time: 234 us; the launch traced here: 233 us
  blocking collectives  156 us (67%)
  starting transfers between devices  31.1 us (13%)
  between operations  13.7 us (6%)
  waiting for transfers between devices  9.4 us (4%)
  Pallas kernels  9.32 us (4%)
  local copies, waits for them, and re-layouts  5.17 us (2%)
  matrix products  4.46 us (2%)
  other arithmetic  3.65 us (2%)
    all_gather x1, blocking collectives, local(): held = lax.all_gather(sent, 'fs', axis=0, tiled=True)  116 us
    all_to_all x1, starting transfers between devices, share_of_sum(): lax.all_to_all(blocks, axis, split_axis=0, concat_axis=0, tiled=True)  18.1 us
    all_gather x1, blocking collectives, local(): return lax.all_gather(out_share, 'tp', axis=0, tiled=True)  14.1 us
    all_gather x1, blocking collectives, local(): rows = lax.all_gather(normed_mid, 'tp', axis=0, tiled=True)  14 us
    ppermute x4, starting transfers between devices, local(): swap = lambda w: lax.ppermute(w, 'grp', [(i, i ^ 1) for i in range(groups)])  13.1 us
    all_to_all x1, blocking collectives, share_of_sum(): lax.all_to_all(blocks, axis, split_axis=0, concat_axis=0, tiled=True)  12 us
    all_to_all x1, waiting for transfers between devices, share_of_sum(): lax.all_to_all(blocks, axis, split_axis=0, concat_axis=0, tiled=True)  8.43 us
    pallas_call x1, Pallas kernels, feed(): pl.pallas_call(functools.partial(feed_body, halves), grid=(2 * halves,),...  5.16 us
  transfers between devices with their start and end apart: 6, of which 3 were waited for; matrix products, arithmetic and copies ran while one was open for 5% of the time, Pallas kernels for 1%

profile of v1, /device:TPU:33, one launch (start us, length us, event | category | flops | bytes accessed | tf_op | source)
XLA Modules:
  0.0 233.2 jit_solution(7054473886614624207)
XLA Ops:
  6.6 1.7 pack.1
  8.3 4.6 %collective-permute-start = (bf16[128,2048]{1,0:T(8,128)(2,1)}, bf16[128,2048]{1,0:T(8,128)(2,1)S(1)}, u32[]{:S(2)}, u32[]{:S(2)}) collective-permute-start(bf16[128,2048]{1,0:T(8,128)(2,1)} %param.16), channel_id=1, source_target_pairs={{0,256},{256,0},{1,257},{257,1},{2,258},{258,2},{3,259},{259,3},{4... | collective-permute-start | bytes 1572872 | tf_op jit(solution)/shard_map/ppermute | solution.py:206
  12.9 0.9 pad_maximum_fusion.1
  13.8 0.9 fusion.51
  14.7 0.9 fusion.49
  15.8 116.3 %all-gather.4 = f16[2048,416]{1,0:T(8,128)(2,1)S(1)} all-gather(f16[64,416]{1,0:T(8,128)(2,1)S(1)} %multiply_convert_fusion.7), channel_id=1, replica_groups=mesh['grp'=2,'fs'=32,'tp'=8] {'fs'}, dimensions={0}, use_global_device_ids=true | all-gather | bytes 1757184 | tf_op jit(solution)/shard_map/all_gather | solution.py:208
  132.1 0.2 fusion.4
  132.3 0.6 fusion.10
  133.0 0.3 multiply_convert_fusion.5
  133.3 0.2 copy.20
  133.6 2.5 %collective-permute-start.1 = (f32[128,224]{1,0:T(8,128)S(1)}, f32[128,224]{1,0:T(8,128)S(1)}, u32[]{:S(2)}, u32[]{:S(2)}) collective-permute-start(f32[128,224]{1,0:T(8,128)S(1)} %copy.17), channel_id=1, source_target_pairs={{0,256},{256,0},{1,257},{257,1},{2,258},{258,2},{3,259},{259,3},{4... | collective-permute-start | bytes 344072 | tf_op jit(solution)/shard_map/ppermute | solution.py:206
  136.1 3.0 %collective-permute-start.2 = (bf16[64,2048]{1,0:T(8,128)(2,1)S(1)}, bf16[64,2048]{1,0:T(8,128)(2,1)S(1)}, u32[]{:S(2)}, u32[]{:S(2)}) collective-permute-start(bf16[64,2048]{1,0:T(8,128)(2,1)S(1)} %bitcast.16), channel_id=1, source_target_pairs={{0,256},{256,0},{1,257},{257,1},{2,258},{258,2},{3,259},{259,3},{4... | collective-permute-start | bytes 786440 | tf_op jit(solution)/shard_map/ppermute | solution.py:206
  139.1 0.2 fusion.7
  139.3 0.6 collective-permute-done.1
  139.9 0.4 broadcast_select_fusion.1
  140.4 2.5 %attend.1 = bf16[128,128]{1,0:T(8,128)(2,1)S(1)} custom-call(f32[128,448]{1,0:T(8,128)S(1)} %pad_maximum_fusion.acc_ref, f32[1,64]{1,0:T(1,128)S(1)} %bitcast.14, f32[64,128]{1,0:T(8,128)S(1)} %bitcast.13, f32[1,128]{1,0:T(1,128)S(1)} %bitcast.15), custom_call_target="tpu_custom_call" | custom-call | flops 40000000 | bytes 500000 | tf_op jit(solution)/shard_map/attend/pallas_call | solution.py:68
  143.0 0.3 fusion.33
  143.3 0.3 collective-permute-done.2
  143.6 1.1 fusion
  144.9 3.0 %collective-permute-start.3 = (bf16[2048,128]{1,0:T(8,128)(2,1)S(1)}, bf16[2048,128]{1,0:T(8,128)(2,1)S(1)}, u32[]{:S(2)}, u32[]{:S(2)}) collective-permute-start(bf16[2048,128]{1,0:T(8,128)(2,1)S(1)} %multiply_convert_fusion.4), channel_id=1, source_target_pairs={{0,256},{256,0},{1,257},{257,1},{2,258},{258,2},{3,259},{259,3},{4... | collective-permute-start | bytes 1572872 | tf_op jit(solution)/shard_map/ppermute | solution.py:206
  147.9 18.1 %all-to-all-start = ((bf16[8,16,2048]{2,1,0:T(8,128)(2,1)}), bf16[8,16,2048]{2,1,0:T(8,128)(2,1)S(1)}, u32[]{:S(2)}, u32[]{:S(2)}) async-start(bf16[8,16,2048]{2,1,0:T(8,128)(2,1)} %bitcast.6), calls=%async_computation | async-start | bytes 1048576 | tf_op jit(solution)/shard_map/all_to_all | solution.py:168
  166.0 1.0 fusion.47
  167.0 8.4 %all-to-all-done = bf16[8,16,2048]{2,1,0:T(8,128)(2,1)S(1)} async-done(((bf16[8,16,2048]{2,1,0:T(8,128)(2,1)}), bf16[8,16,2048]{2,1,0:T(8,128)(2,1)S(1)}, u32[]{:S(2)}, u32[]{:S(2)}) %all-to-all-start) | async-done | bytes 524320 | tf_op jit(solution)/shard_map/all_to_all | solution.py:168
  175.6 0.2 multiply_reduce_fusion.1
  176.0 14.0 %all_gather.13.rows_ref = bf16[128,2048]{1,0:T(8,128)(2,1)S(1)} all-gather(bf16[16,2048]{1,0:T(8,128)(2,1)S(1)} %multiply_convert_fusion.6), channel_id=1, replica_groups=mesh['grp'=2,'fs'=32,'tp'=8] {'tp'}, dimensions={0}, use_global_device_ids=true | all-gather | bytes 589824 | tf_op jit(solution)/shard_map/all_gather | solution.py:246
  189.9 1.1 fusion.48
  191.1 2.0 fusion.3.part_ref
  193.1 5.2 %feed.1 = bf16[128,2048]{1,0:T(8,128)(2,1)S(1)} custom-call(bf16[128,2048]{1,0:T(8,128)(2,1)S(1)} %all_gather.13.rows_ref, bf16[2048,1792]{1,0:T(8,128)(2,1)} %all-gather.3.cloned.1.call-done.weight_ref, f32[128,2048]{1,0:T(8,128)S(1)} %fusion.3.part_ref), custom_call_target="tpu_custom_call" | custom-call | flops 939524096 | bytes 7340032 | tf_op jit(solution)/shard_map/feed/pallas_call | solution.py:110
  198.3 12.0 %all_to_all.10 = bf16[8,16,2048]{2,1,0:T(8,128)(2,1)S(1)} all-to-all(bf16[8,16,2048]{2,1,0:T(8,128)(2,1)S(1)} %bitcast.12), channel_id=1, replica_groups=mesh['grp'=2,'fs'=32,'tp'=8] {'tp'}, dimensions={0} | all-to-all | bytes 1048576 | tf_op jit(solution)/shard_map/all_to_all | solution.py:168
  210.5 1.0 add_convert_fusion
  211.5 14.1 %all_gather.15 = bf16[128,2048]{1,0:T(8,128)(2,1)S(1)} all-gather(bf16[16,2048]{1,0:T(8,128)(2,1)S(1)} %add_convert_fusion), channel_id=1, replica_groups=mesh['grp'=2,'fs'=32,'tp'=8] {'tp'}, dimensions={0}, use_global_device_ids=true | all-gather | bytes 589824 | tf_op jit(solution)/shard_map/all_gather | solution.py:251
  225.5 0.8 copy.23
  (38 shorter events, 1.2 us)
Async XLA Ops:
  6.5 186.6 %all-gather.3.cloned.1.call-start = ((), (), s32[]{:S(2)}) async-start(), calls=%async_computation.2 | async-start | bytes 7569408 | tf_op jit(solution)/shard_map/all_gather | solution.py:192
  6.6 125.7 %copy-start.8 = (f32[2048]{0:T(1024)S(1)}, f32[2048]{0:T(1024)}, u32[]{:S(2)}) copy-start(f32[2048]{0:T(1024)} %param.17) | copy-start | bytes 24580
  8.3 123.8 %collective-permute-start = (bf16[128,2048]{1,0:T(8,128)(2,1)}, bf16[128,2048]{1,0:T(8,128)(2,1)S(1)}, u32[]{:S(2)}, u32[]{:S(2)}) collective-permute-start(bf16[128,2048]{1,0:T(8,128)(2,1)} %param.16), channel_id=1, source_target_pairs={{0,256},{256,0},{1,257},{257,1},{2,258},{258,2},{3,259},{259,3},{4... | collective-permute-start | bytes 1572872 | tf_op jit(solution)/shard_map/ppermute | solution.py:206
  132.3 6.8 %copy-start.4 = (bf16[128,2048]{1,0:T(8,128)(2,1)S(1)}, bf16[128,2048]{1,0:T(8,128)(2,1)}, u32[]{:S(2)}) copy-start(bf16[128,2048]{1,0:T(8,128)(2,1)} %param.16) | copy-start | bytes 1572868
  133.5 6.9 %copy-start = (f32[128,64]{0,1:T(8,128)S(1)}, f32[128,64]{0,1:T(8,128)}, u32[]{:S(2)}) copy-start(f32[128,64]{0,1:T(8,128)} %param.24) | copy-start | bytes 98308
  133.6 6.9 %copy-start.1 = (f32[64]{0:T(128)S(1)}, f32[64]{0:T(128)}, u32[]{:S(2)}) copy-start(f32[64]{0:T(128)} %param.23) | copy-start | bytes 772
  133.6 6.9 %copy-start.2 = (f32[128]{0:T(128)S(1)}, f32[128]{0:T(128)}, u32[]{:S(2)}) copy-start(f32[128]{0:T(128)} %param.25) | copy-start | bytes 1540
  133.6 6.3 %collective-permute-start.1 = (f32[128,224]{1,0:T(8,128)S(1)}, f32[128,224]{1,0:T(8,128)S(1)}, u32[]{:S(2)}, u32[]{:S(2)}) collective-permute-start(f32[128,224]{1,0:T(8,128)S(1)} %copy.17), channel_id=1, source_target_pairs={{0,256},{256,0},{1,257},{257,1},{2,258},{258,2},{3,259},{259,3},{4... | collective-permute-start | bytes 344072 | tf_op jit(solution)/shard_map/ppermute | solution.py:206
  136.1 7.5 %collective-permute-start.2 = (bf16[64,2048]{1,0:T(8,128)(2,1)S(1)}, bf16[64,2048]{1,0:T(8,128)(2,1)S(1)}, u32[]{:S(2)}, u32[]{:S(2)}) collective-permute-start(bf16[64,2048]{1,0:T(8,128)(2,1)S(1)} %bitcast.16), channel_id=1, source_target_pairs={{0,256},{256,0},{1,257},{257,1},{2,258},{258,2},{3,259},{259,3},{4... | collective-permute-start | bytes 786440 | tf_op jit(solution)/shard_map/ppermute | solution.py:206
  144.9 30.8 %copy-start.5 = (f32[2048]{0:T(1024)S(1)}, f32[2048]{0:T(1024)}, u32[]{:S(2)}) copy-start(f32[2048]{0:T(1024)} %param.27) | copy-start | bytes 24580
  144.9 31.0 %copy-start.6 = (f32[2048]{0:T(1024)S(1)}, f32[2048]{0:T(1024)}, u32[]{:S(2)}) copy-start(f32[2048]{0:T(1024)} %param.28) | copy-start | bytes 24580
  144.9 45.1 %collective-permute-start.3 = (bf16[2048,128]{1,0:T(8,128)(2,1)S(1)}, bf16[2048,128]{1,0:T(8,128)(2,1)S(1)}, u32[]{:S(2)}, u32[]{:S(2)}) collective-permute-start(bf16[2048,128]{1,0:T(8,128)(2,1)S(1)} %multiply_convert_fusion.4), channel_id=1, source_target_pairs={{0,256},{256,0},{1,257},{257,1},{2,258},{258,2},{3,259},{259,3},{4... | collective-permute-start | bytes 1572872 | tf_op jit(solution)/shard_map/ppermute | solution.py:206
  147.9 27.5 %all-to-all-start = ((bf16[8,16,2048]{2,1,0:T(8,128)(2,1)}), bf16[8,16,2048]{2,1,0:T(8,128)(2,1)S(1)}, u32[]{:S(2)}, u32[]{:S(2)}) async-start(bf16[8,16,2048]{2,1,0:T(8,128)(2,1)} %bitcast.6), calls=%async_computation | async-start | bytes 1048576 | tf_op jit(solution)/shard_map/all_to_all | solution.py:168
  189.9 1.1 copy-start.3
  193.1 17.4 %copy-start.7 = (f32[2048]{0:T(1024)S(1)}, f32[2048]{0:T(1024)}, u32[]{:S(2)}) copy-start(f32[2048]{0:T(1024)} %param.29) | copy-start | bytes 24580
Sparse Core Ops, SparseCore 0:
  9.4 165.9 all-gather.2

commit v2 on v1

--- a/solution.py
+++ b/solution.py
@@ -215,6 +215,9 @@
     )
     acc_far = swap(sent_home)
     tokens, held, sent_home = lax.optimization_barrier((tokens, held, sent_home))
+    share = tokens.shape[0] // lax.axis_size("tp")
+    own_tokens = lax.dynamic_slice_in_dim(tokens, lax.axis_index("tp") * share, share, 0)
+    own_tokens = lax.optimization_barrier(own_tokens.astype(F32))
     acc_near = jnp.dot(
         normed(tokens), unscaled(held, edges[2], edges[3]), preferred_element_type=F32
     )
@@ -239,9 +242,7 @@
         jnp.concatenate([w[:, lo:hi] for w in (apart_near, apart_far)], 1)
         for lo, hi in zip(edges[:2], edges[1:3])
     )
-    share = mixed.shape[0]
-    own_tokens = lax.dynamic_slice_in_dim(tokens, lax.axis_index("tp") * share, share, 0)
-    stream = own_tokens.astype(F32) + root_norm(mixed, post_attention_gain)
+    stream = own_tokens + root_norm(mixed, post_attention_gain)
     normed_mid = root_norm(stream, pre_feedforward_gain).astype(BF16)
     rows = lax.all_gather(normed_mid, "tp", axis=0, tiled=True)
     act = jnp.square(jax.nn.relu(jnp.dot(rows, up_apart, preferred_element_type=F32))).astype(BF16)

time: 234 us -> 234 us (level)
  transfers between devices with their start and end apart: 6 -> 6, of which waited for: 3 -> 2; matrix products, arithmetic and copies ran while one was open for 5% -> 5% of each run, Pallas kernels for 1% -> 1%
where the time goes in v2:
time: 234 us; the launch traced here: 233 us
  blocking collectives  155 us (66%)
  starting transfers between devices  32.2 us (14%)
  between operations  13.7 us (6%)
  waiting for transfers between devices  9.37 us (4%)
  Pallas kernels  9.31 us (4%)
  matrix products  5.21 us (2%)
  local copies, waits for them, and re-layouts  4.85 us (2%)
  other arithmetic  2.79 us (1%)
    all_gather x1, blocking collectives, local(): held = lax.all_gather(sent, 'fs', axis=0, tiled=True)  115 us
    all_to_all x1, starting transfers between devices, share_of_sum(): lax.all_to_all(blocks, axis, split_axis=0, concat_axis=0, tiled=True)  19.3 us
    all_gather x1, blocking collectives, local(): return lax.all_gather(out_share, 'tp', axis=0, tiled=True)  14.1 us
    all_gather x1, blocking collectives, local(): rows = lax.all_gather(normed_mid, 'tp', axis=0, tiled=True)  14 us
    ppermute x4, starting transfers between devices, local(): swap = lambda w: lax.ppermute(w, 'grp', [(i, i ^ 1) for i in range(groups)])  12.9 us
    all_to_all x1, blocking collectives, share_of_sum(): lax.all_to_all(blocks, axis, split_axis=0, concat_axis=0, tiled=True)  12 us
    all_to_all x1, waiting for transfers between devices, share_of_sum(): lax.all_to_all(blocks, axis, split_axis=0, concat_axis=0, tiled=True)  9.14 us
    pallas_call x1, Pallas kernels, feed(): pl.pallas_call(functools.partial(feed_body, halves), grid=(2 * halves,),...  5.15 us
  transfers between devices with their start and end apart: 6, of which 2 were waited for; matrix products, arithmetic and copies ran while one was open for 5% of the time, Pallas kernels for 1%

profile of v2, /device:TPU:33, one launch (start us, length us, event | category | flops | bytes accessed | tf_op | source)
XLA Modules:
  0.0 232.9 jit_solution(7100423709145017661)
XLA Ops:
  6.6 1.7 pack.1
  8.3 4.6 %collective-permute-start = (bf16[128,2048]{1,0:T(8,128)(2,1)}, bf16[128,2048]{1,0:T(8,128)(2,1)S(1)}, u32[]{:S(2)}, u32[]{:S(2)}) collective-permute-start(bf16[128,2048]{1,0:T(8,128)(2,1)} %param.16), channel_id=1, source_target_pairs={{0,256},{256,0},{1,257},{257,1},{2,258},{258,2},{3,259},{259,3},{4... | collective-permute-start | bytes 1572872 | tf_op jit(solution)/shard_map/ppermute | solution.py:206
  12.9 0.9 pad_maximum_fusion.1
  13.8 0.9 fusion.51
  14.7 0.9 fusion.49
  15.6 0.1 concatenate.21
  15.8 115.4 %all-gather.4 = f16[2048,416]{1,0:T(8,128)(2,1)S(1)} all-gather(f16[64,416]{1,0:T(8,128)(2,1)S(1)} %multiply_convert_fusion.7), channel_id=1, replica_groups=mesh['grp'=2,'fs'=32,'tp'=8] {'fs'}, dimensions={0}, use_global_device_ids=true | all-gather | bytes 1757184 | tf_op jit(solution)/shard_map/all_gather | solution.py:208
  131.2 0.2 fusion.4
  131.4 0.6 fusion.10
  132.0 0.8 copy.17
  132.8 2.5 %collective-permute-start.1 = (f32[128,224]{1,0:T(8,128)}, f32[128,224]{1,0:T(8,128)}, u32[]{:S(2)}, u32[]{:S(2)}) collective-permute-start(f32[128,224]{1,0:T(8,128)} %copy.17), channel_id=1, source_target_pairs={{0,256},{256,0},{1,257},{257,1},{2,258},{258,2},{3,259},{259,3},{4... | collective-permute-start | bytes 344072 | tf_op jit(solution)/shard_map/ppermute | solution.py:206
  135.3 0.3 multiply_convert_fusion.5
  135.6 0.2 copy.20
  135.9 2.9 %collective-permute-start.2 = (bf16[64,2048]{1,0:T(8,128)(2,1)S(1)}, bf16[64,2048]{1,0:T(8,128)(2,1)S(1)}, u32[]{:S(2)}, u32[]{:S(2)}) collective-permute-start(bf16[64,2048]{1,0:T(8,128)(2,1)S(1)} %bitcast.16), channel_id=1, source_target_pairs={{0,256},{256,0},{1,257},{257,1},{2,258},{258,2},{3,259},{259,3},{4... | collective-permute-start | bytes 786440 | tf_op jit(solution)/shard_map/ppermute | solution.py:206
  138.9 0.2 fusion.7
  139.1 1.3 broadcast_select_fusion.1
  140.6 2.5 %attend.1 = bf16[128,128]{1,0:T(8,128)(2,1)S(1)} custom-call(f32[128,448]{1,0:T(8,128)S(1)} %pad_maximum_fusion.acc_ref, f32[1,64]{1,0:T(1,128)S(1)} %bitcast.14, f32[64,128]{1,0:T(8,128)S(1)} %bitcast.13, f32[1,128]{1,0:T(1,128)S(1)} %bitcast.15), custom_call_target="tpu_custom_call" | custom-call | flops 40000000 | bytes 500000 | tf_op jit(solution)/shard_map/attend/pallas_call | solution.py:68
  143.1 0.3 fusion.33
  143.6 1.1 fusion
  144.8 2.8 %collective-permute-start.3 = (bf16[2048,128]{1,0:T(8,128)(2,1)S(1)}, bf16[2048,128]{1,0:T(8,128)(2,1)S(1)}, u32[]{:S(2)}, u32[]{:S(2)}) collective-permute-start(bf16[2048,128]{1,0:T(8,128)(2,1)S(1)} %multiply_convert_fusion.4), channel_id=1, source_target_pairs={{0,256},{256,0},{1,257},{257,1},{2,258},{258,2},{3,259},{259,3},{4... | collective-permute-start | bytes 1572872 | tf_op jit(solution)/shard_map/ppermute | solution.py:206
  147.6 19.3 %all-to-all-start = ((bf16[8,16,2048]{2,1,0:T(8,128)(2,1)}), bf16[8,16,2048]{2,1,0:T(8,128)(2,1)S(1)}, u32[]{:S(2)}, u32[]{:S(2)}) async-start(bf16[8,16,2048]{2,1,0:T(8,128)(2,1)} %bitcast.6), calls=%async_computation | async-start | bytes 1048576 | tf_op jit(solution)/shard_map/all_to_all | solution.py:168
  167.0 0.2 fusion.47
  167.2 9.1 %all-to-all-done = bf16[8,16,2048]{2,1,0:T(8,128)(2,1)S(1)} async-done(((bf16[8,16,2048]{2,1,0:T(8,128)(2,1)}), bf16[8,16,2048]{2,1,0:T(8,128)(2,1)S(1)}, u32[]{:S(2)}, u32[]{:S(2)}) %all-to-all-start) | async-done | bytes 524320 | tf_op jit(solution)/shard_map/all_to_all | solution.py:168
  176.4 0.1 multiply_reduce_fusion.2
  176.5 0.2 multiply_reduce_fusion.1
  176.9 14.0 %all_gather.13.rows_ref = bf16[128,2048]{1,0:T(8,128)(2,1)S(1)} all-gather(bf16[16,2048]{1,0:T(8,128)(2,1)S(1)} %multiply_convert_fusion.6), channel_id=1, replica_groups=mesh['grp'=2,'fs'=32,'tp'=8] {'tp'}, dimensions={0}, use_global_device_ids=true | all-gather | bytes 589824 | tf_op jit(solution)/shard_map/all_gather | solution.py:247
  190.9 1.0 fusion.48
  191.8 1.8 fusion.3.part_ref
  193.7 5.1 %feed.1 = bf16[128,2048]{1,0:T(8,128)(2,1)S(1)} custom-call(bf16[128,2048]{1,0:T(8,128)(2,1)S(1)} %all_gather.13.rows_ref, bf16[2048,1792]{1,0:T(8,128)(2,1)} %all-gather.3.cloned.1.call-done.weight_ref, f32[128,2048]{1,0:T(8,128)S(1)} %fusion.3.part_ref), custom_call_target="tpu_custom_call" | custom-call | flops 939524096 | bytes 7340032 | tf_op jit(solution)/shard_map/feed/pallas_call | solution.py:110
  198.8 12.0 %all_to_all.10 = bf16[8,16,2048]{2,1,0:T(8,128)(2,1)S(1)} all-to-all(bf16[8,16,2048]{2,1,0:T(8,128)(2,1)S(1)} %bitcast.12), channel_id=1, replica_groups=mesh['grp'=2,'fs'=32,'tp'=8] {'tp'}, dimensions={0} | all-to-all | bytes 1048576 | tf_op jit(solution)/shard_map/all_to_all | solution.py:168
  211.2 14.1 %all_gather.15 = bf16[128,2048]{1,0:T(8,128)(2,1)S(1)} all-gather(bf16[16,2048]{1,0:T(8,128)(2,1)S(1)} %add_convert_fusion), channel_id=1, replica_groups=mesh['grp'=2,'fs'=32,'tp'=8] {'tp'}, dimensions={0}, use_global_device_ids=true | all-gather | bytes 589824 | tf_op jit(solution)/shard_map/all_gather | solution.py:252
  225.3 0.8 copy.23
  (37 shorter events, 1.1 us)
Async XLA Ops:
  6.5 187.1 %all-gather.3.cloned.1.call-start = ((), (), s32[]{:S(2)}) async-start(), calls=%async_computation.2 | async-start | bytes 7569408 | tf_op jit(solution)/shard_map/all_gather | solution.py:192
  6.6 124.8 %copy-start.7 = (f32[2048]{0:T(1024)S(1)}, f32[2048]{0:T(1024)}, u32[]{:S(2)}) copy-start(f32[2048]{0:T(1024)} %param.17) | copy-start | bytes 24580
  8.3 122.9 %collective-permute-start = (bf16[128,2048]{1,0:T(8,128)(2,1)}, bf16[128,2048]{1,0:T(8,128)(2,1)S(1)}, u32[]{:S(2)}, u32[]{:S(2)}) collective-permute-start(bf16[128,2048]{1,0:T(8,128)(2,1)} %param.16), channel_id=1, source_target_pairs={{0,256},{256,0},{1,257},{257,1},{2,258},{258,2},{3,259},{259,3},{4... | collective-permute-start | bytes 1572872 | tf_op jit(solution)/shard_map/ppermute | solution.py:206
  131.4 7.4 %copy-start.3 = (bf16[128,2048]{1,0:T(8,128)(2,1)S(1)}, bf16[128,2048]{1,0:T(8,128)(2,1)}, u32[]{:S(2)}) copy-start(bf16[128,2048]{1,0:T(8,128)(2,1)} %param.16) | copy-start | bytes 1572868
  132.8 6.3 %collective-permute-start.1 = (f32[128,224]{1,0:T(8,128)}, f32[128,224]{1,0:T(8,128)}, u32[]{:S(2)}, u32[]{:S(2)}) collective-permute-start(f32[128,224]{1,0:T(8,128)} %copy.17), channel_id=1, source_target_pairs={{0,256},{256,0},{1,257},{257,1},{2,258},{258,2},{3,259},{259,3},{4... | collective-permute-start | bytes 344072 | tf_op jit(solution)/shard_map/ppermute | solution.py:206
  135.8 4.7 %copy-start = (f32[128,64]{0,1:T(8,128)S(1)}, f32[128,64]{0,1:T(8,128)}, u32[]{:S(2)}) copy-start(f32[128,64]{0,1:T(8,128)} %param.24) | copy-start | bytes 98308
  135.9 4.7 %copy-start.1 = (f32[64]{0:T(128)S(1)}, f32[64]{0:T(128)}, u32[]{:S(2)}) copy-start(f32[64]{0:T(128)} %param.23) | copy-start | bytes 772
  135.9 4.7 %copy-start.2 = (f32[128]{0:T(128)S(1)}, f32[128]{0:T(128)}, u32[]{:S(2)}) copy-start(f32[128]{0:T(128)} %param.25) | copy-start | bytes 1540
  135.9 7.7 %collective-permute-start.2 = (bf16[64,2048]{1,0:T(8,128)(2,1)S(1)}, bf16[64,2048]{1,0:T(8,128)(2,1)S(1)}, u32[]{:S(2)}, u32[]{:S(2)}) collective-permute-start(bf16[64,2048]{1,0:T(8,128)(2,1)S(1)} %bitcast.16), channel_id=1, source_target_pairs={{0,256},{256,0},{1,257},{257,1},{2,258},{258,2},{3,259},{259,3},{4... | collective-permute-start | bytes 786440 | tf_op jit(solution)/shard_map/ppermute | solution.py:206
  144.8 31.7 %copy-start.4 = (f32[2048]{0:T(1024)S(1)}, f32[2048]{0:T(1024)}, u32[]{:S(2)}) copy-start(f32[2048]{0:T(1024)} %param.27) | copy-start | bytes 24580
  144.8 46.0 %collective-permute-start.3 = (bf16[2048,128]{1,0:T(8,128)(2,1)S(1)}, bf16[2048,128]{1,0:T(8,128)(2,1)S(1)}, u32[]{:S(2)}, u32[]{:S(2)}) collective-permute-start(bf16[2048,128]{1,0:T(8,128)(2,1)S(1)} %multiply_convert_fusion.4), channel_id=1, source_target_pairs={{0,256},{256,0},{1,257},{257,1},{2,258},{258,2},{3,259},{259,3},{4... | collective-permute-start | bytes 1572872 | tf_op jit(solution)/shard_map/ppermute | solution.py:206
  147.6 29.1 %copy-start.5 = (f32[2048]{0:T(1024)S(1)}, f32[2048]{0:T(1024)}, u32[]{:S(2)}) copy-start(f32[2048]{0:T(1024)} %param.28) | copy-start | bytes 24580
  147.6 28.7 %all-to-all-start = ((bf16[8,16,2048]{2,1,0:T(8,128)(2,1)}), bf16[8,16,2048]{2,1,0:T(8,128)(2,1)S(1)}, u32[]{:S(2)}, u32[]{:S(2)}) async-start(bf16[8,16,2048]{2,1,0:T(8,128)(2,1)} %bitcast.6), calls=%async_computation | async-start | bytes 1048576 | tf_op jit(solution)/shard_map/all_to_all | solution.py:168
  193.6 17.5 %copy-start.6 = (f32[2048]{0:T(1024)S(1)}, f32[2048]{0:T(1024)}, u32[]{:S(2)}) copy-start(f32[2048]{0:T(1024)} %param.29) | copy-start | bytes 24580
Sparse Core Ops, SparseCore 0:
  9.4 166.2 all-gather.2

commit v3 on v2

--- a/solution.py
+++ b/solution.py
@@ -74,7 +74,9 @@
     )(acc, bias, extra, gain)
 
 
-def feed_body(halves, rows_ref, weight_ref, part_ref, out_ref, sum_ref, act_ref):
+def feed_body(
+    halves, rows_ref, weight_ref, last_ref, early_ref, part_ref, out_ref, sum_ref, act_ref
+):
     step = pl.program_id(0)
 
     @pl.when(step < halves)
@@ -98,12 +100,16 @@
         product = lax.dot_general(
             act_ref[...], weight_ref[...], (((1,), (1,)), ((), ())), preferred_element_type=F32
         )
+        product += lax.dot_general(
+            early_ref[...], last_ref[...], (((1,), (1,)), ((), ())), preferred_element_type=F32
+        )
         out_ref[...] = (product + part_ref[...]).astype(out_ref.dtype)
 
 
-def feed(rows, both, part):
+def feed(rows, both, early, part):
     length, width = rows.shape
-    units = both.shape[1] // 2
+    count = early.shape[1]
+    units = (both.shape[1] - count) // 2
     halves = 2
     block = width // halves
     later = lambda s: (0, jnp.maximum(s - halves, 0))
@@ -113,6 +119,10 @@
         in_specs=[
             pl.BlockSpec((length, block), lambda s: (0, jnp.minimum(s, halves - 1))),
             pl.BlockSpec((block, units), lambda s: (lax.rem(s, halves), s // halves)),
+            pl.BlockSpec(
+                (block, count), lambda s: (jnp.maximum(s - halves, 0), 2 * units // count)
+            ),
+            pl.BlockSpec((length, count), lambda s: (0, 0)),
             pl.BlockSpec((length, block), later),
         ],
         out_specs=pl.BlockSpec((length, block), later),
@@ -125,20 +135,29 @@
             flops=4 * length * width * units, bytes_accessed=4 * width * units, transcendentals=0
         ),
         name="feed",
-    )(rows, both, part)
+    )(rows, both, both, early, part)
 
 
 def pack_body(first, up_ref, down_ref, out_ref, held, arrived, left):
-    width = up_ref.shape[1] - first
+    most = up_ref.shape[1] - 2 * first
+    plan = (
+        (up_ref, 2 * first, most, 0),
+        (down_ref, 2 * first, most, most),
+        (down_ref, first, first, 2 * most),
+    )
     brought = []
-    for i, source in enumerate((up_ref, down_ref)):
-        copy = pltpu.make_async_copy(source.at[:, pl.ds(first, width)], held.at[i], arrived.at[i])
+    for i, (source, at, width, to) in enumerate(plan):
+        copy = pltpu.make_async_copy(
+            source.at[:, pl.ds(at, width)], held.at[:, pl.ds(to, width)], arrived.at[i]
+        )
         copy.start()
         brought.append(copy)
     sent = []
-    for i, copy in enumerate(brought):
-        copy.wait()
-        out = pltpu.make_async_copy(held.at[i], out_ref.at[:, pl.ds(i * width, width)], left.at[i])
+    for i, (source, at, width, to) in enumerate(plan):
+        brought[i].wait()
+        out = pltpu.make_async_copy(
+            held.at[:, pl.ds(to, width)], out_ref.at[:, pl.ds(to, width)], left.at[i]
+        )
         out.start()
         sent.append(out)
     for out in sent:
@@ -146,16 +165,16 @@
 
 
 def pack(up, down, first):
-    depth, width = up.shape[0], up.shape[1] - first
+    shape = (up.shape[0], 2 * up.shape[1] - 3 * first)
     return pl.pallas_call(
         functools.partial(pack_body, first),
         in_specs=[pl.BlockSpec(memory_space=pltpu.HBM)] * 2,
         out_specs=pl.BlockSpec(memory_space=pltpu.HBM),
-        out_shape=jax.ShapeDtypeStruct((depth, 2 * width), up.dtype),
+        out_shape=jax.ShapeDtypeStruct(shape, up.dtype),
         scratch_shapes=[
-            pltpu.VMEM((2, depth, width), up.dtype),
-            pltpu.SemaphoreType.DMA((2,)),
-            pltpu.SemaphoreType.DMA((2,)),
+            pltpu.VMEM(shape, up.dtype),
+            pltpu.SemaphoreType.DMA((3,)),
+            pltpu.SemaphoreType.DMA((3,)),
         ],
         compiler_params=pltpu.CompilerParams(vmem_limit_bytes=62 * 2**20),
         name="pack",
@@ -196,7 +215,7 @@
     projections = jnp.concatenate(
         [value_weight, output_gate_weight, query_weight, key_weight, decay_weight], 1
     )
-    parts = (up_weight[:, :apart], down_rows[:, :apart], projections, attention_out_weight.T)
+    parts = (up_weight[:, : 2 * apart], down_rows[:, :apart], projections, attention_out_weight.T)
     sizes = [p.shape[1] // 2 for p in parts]
     halves = [p[:, h * n : (h + 1) * n] for h in range(2) for p, n in zip(parts, sizes)]
     half = lax.dynamic_slice_in_dim(
@@ -246,8 +265,12 @@
     normed_mid = root_norm(stream, pre_feedforward_gain).astype(BF16)
     rows = lax.all_gather(normed_mid, "tp", axis=0, tiled=True)
     act = jnp.square(jax.nn.relu(jnp.dot(rows, up_apart, preferred_element_type=F32))).astype(BF16)
+    own, other = act[:, :apart], act[:, apart:]
+    early = jnp.where(first, other, own)
+    act = jnp.where(first, own, other)
+    act = jnp.where(first, act, jnp.roll(act, sizes[1], 1))
     part = lax.dot_general(act, down_apart, (((1,), (1,)), ((), ())), preferred_element_type=F32)
-    feed_share = share_of_sum(feed(rows, both, part), "tp")
+    feed_share = share_of_sum(feed(rows, both, early, part), "tp")
     out_share = (stream + root_norm(feed_share, post_feedforward_gain)).astype(BF16)
     return lax.all_gather(out_share, "tp", axis=0, tiled=True)
 

time: 234 us -> 234 us (level)
  waiting for transfers between devices: 9.37 us -> 4.14 us
  local copies, waits for them, and re-layouts: 4.85 us -> 8.46 us
  blocking collectives: 155 us -> 158 us
  starting transfers between devices: 32.2 us -> 29.5 us
    all_to_all x1, waiting for transfers between devices: 9.14 us -> 3.78 us  [share_of_sum(): lax.all_to_all(blocks, axis, split_axis=0, concat_axis=0, tiled=True)]
    all_to_all x1, starting transfers between devices: 19.3 us -> 16.7 us  [share_of_sum(): lax.all_to_all(blocks, axis, split_axis=0, concat_axis=0, tiled=True)]
    all_to_all x1, blocking collectives: 12 us -> 14.4 us  [share_of_sum(): lax.all_to_all(blocks, axis, split_axis=0, concat_axis=0, tiled=True)]
  transfers between devices with their start and end apart: 6 -> 6, of which waited for: 2 -> 2; matrix products, arithmetic and copies ran while one was open for 5% -> 7% of each run, Pallas kernels for 1% -> 1%
where the time goes in v3:
time: 234 us; the launch traced here: 233 us
  blocking collectives  158 us (68%)
  starting transfers between devices  29.5 us (13%)
  between operations  13.8 us (6%)
  Pallas kernels  9.15 us (4%)
  local copies, waits for them, and re-layouts  8.46 us (4%)
  matrix products  5.3 us (2%)
  other arithmetic  4.15 us (2%)
  waiting for transfers between devices  4.14 us (2%)
    all_gather x1, blocking collectives, local(): held = lax.all_gather(sent, 'fs', axis=0, tiled=True)  116 us
    all_to_all x1, starting transfers between devices, share_of_sum(): lax.all_to_all(blocks, axis, split_axis=0, concat_axis=0, tiled=True)  16.7 us
    all_to_all x1, blocking collectives, share_of_sum(): lax.all_to_all(blocks, axis, split_axis=0, concat_axis=0, tiled=True)  14.4 us
    all_gather x1, blocking collectives, local(): rows = lax.all_gather(normed_mid, 'tp', axis=0, tiled=True)  14.1 us
    all_gather x1, blocking collectives, local(): return lax.all_gather(out_share, 'tp', axis=0, tiled=True)  14.1 us
    ppermute x4, starting transfers between devices, local(): swap = lambda w: lax.ppermute(w, 'grp', [(i, i ^ 1) for i in range(groups)])  12.8 us
    pallas_call x1, Pallas kernels, feed(): pl.pallas_call(functools.partial(feed_body, halves), grid=(2 * halves,),...  4.99 us
  transfers between devices with their start and end apart: 6, of which 2 were waited for; matrix products, arithmetic and copies ran while one was open for 7% of the time, Pallas kernels for 1%

profile of v3, /device:TPU:33, one launch (start us, length us, event | category | flops | bytes accessed | tf_op | source)
XLA Modules:
  0.0 233.0 jit_solution(10250945211301854655)
XLA Ops:
  6.6 1.7 pack.1
  8.3 4.6 %collective-permute-start = (bf16[128,2048]{1,0:T(8,128)(2,1)}, bf16[128,2048]{1,0:T(8,128)(2,1)S(1)}, u32[]{:S(2)}, u32[]{:S(2)}) collective-permute-start(bf16[128,2048]{1,0:T(8,128)(2,1)} %param.16), channel_id=1, source_target_pairs={{0,256},{256,0},{1,257},{257,1},{2,258},{258,2},{3,259},{259,3},{4... | collective-permute-start | bytes 1572872 | tf_op jit(solution)/shard_map/ppermute | solution.py:225
  12.9 0.9 pad_maximum_fusion.1
  13.8 0.9 fusion.45
  14.7 0.7 fusion.46
  15.4 0.9 fusion.48
  16.5 115.9 %all-gather.4 = f16[2048,480]{1,0:T(8,128)(2,1)S(1)} all-gather(f16[64,480]{1,0:T(8,128)(2,1)S(1)} %multiply_convert_fusion.7), channel_id=1, replica_groups=mesh['grp'=2,'fs'=32,'tp'=8] {'fs'}, dimensions={0}, use_global_device_ids=true | all-gather | bytes 2027520 | tf_op jit(solution)/shard_map/all_gather | solution.py:227
  132.6 1.3 fusion.9
  134.0 0.8 copy.21
  134.8 1.9 collective-permute-start.1
  136.7 0.3 multiply_convert_fusion.5
  137.3 3.5 %collective-permute-start.2 = (bf16[64,2048]{1,0:T(8,128)(2,1)S(1)}, bf16[64,2048]{1,0:T(8,128)(2,1)S(1)}, u32[]{:S(2)}, u32[]{:S(2)}) collective-permute-start(bf16[64,2048]{1,0:T(8,128)(2,1)S(1)} %bitcast.16), channel_id=1, source_target_pairs={{0,256},{256,0},{1,257},{257,1},{2,258},{258,2},{3,259},{259,3},{4... | collective-permute-start | bytes 786440 | tf_op jit(solution)/shard_map/ppermute | solution.py:225
  141.1 1.7 broadcast_select_fusion.1
  143.0 2.5 %attend.1 = bf16[128,128]{1,0:T(8,128)(2,1)S(1)} custom-call(f32[128,448]{1,0:T(8,128)S(1)} %pad_maximum_fusion.acc_ref, f32[1,64]{1,0:T(1,128)S(1)} %bitcast.14, f32[64,128]{1,0:T(8,128)S(1)} %bitcast.13, f32[1,128]{1,0:T(1,128)S(1)} %bitcast.15), custom_call_target="tpu_custom_call" | custom-call | flops 40000000 | bytes 500000 | tf_op jit(solution)/shard_map/attend/pallas_call | solution.py:68
  145.5 0.3 fusion.31
  145.8 1.1 fusion
  147.0 16.7 %all-to-all-start = ((bf16[8,16,2048]{2,1,0:T(8,128)(2,1)}), bf16[8,16,2048]{2,1,0:T(8,128)(2,1)S(1)}, u32[]{:S(2)}, u32[]{:S(2)}) async-start(bf16[8,16,2048]{2,1,0:T(8,128)(2,1)} %bitcast.6), calls=%async_computation | async-start | bytes 1048576 | tf_op jit(solution)/shard_map/all_to_all | solution.py:187
  163.6 1.5 multiply_convert_fusion
  165.1 1.3 copy.25
  166.5 2.7 %collective-permute-start.3 = (bf16[2048,192]{0,1:T(8,128)(2,1)}, bf16[2048,192]{0,1:T(8,128)(2,1)}, u32[]{:S(2)}, u32[]{:S(2)}) collective-permute-start(bf16[2048,192]{0,1:T(8,128)(2,1)} %copy.25), channel_id=1, source_target_pairs={{0,256},{256,0},{1,257},{257,1},{2,258},{258,2},{3,259},{259,3},{4... | collective-permute-start | bytes 2359304 | tf_op jit(solution)/shard_map/ppermute | solution.py:225
  169.2 3.8 %all-to-all-done = bf16[8,16,2048]{2,1,0:T(8,128)(2,1)S(1)} async-done(((bf16[8,16,2048]{2,1,0:T(8,128)(2,1)}), bf16[8,16,2048]{2,1,0:T(8,128)(2,1)S(1)}, u32[]{:S(2)}, u32[]{:S(2)}) %all-to-all-start) | async-done | bytes 524320 | tf_op jit(solution)/shard_map/all_to_all | solution.py:187
  173.5 14.1 %all_gather.13.rows_ref = bf16[128,2048]{1,0:T(8,128)(2,1)S(1)} all-gather(bf16[16,2048]{1,0:T(8,128)(2,1)S(1)} %multiply_convert_fusion.6), channel_id=1, replica_groups=mesh['grp'=2,'fs'=32,'tp'=8] {'tp'}, dimensions={0}, use_global_device_ids=true | all-gather | bytes 589824 | tf_op jit(solution)/shard_map/all_gather | solution.py:266
  187.9 1.1 slice.105
  189.0 0.3 copy.29
  189.3 1.0 slice.111
  190.3 0.3 copy.30
  190.6 0.3 fusion.2
  191.0 0.5 fusion.20.part_ref
  191.5 5.0 %feed.1 = bf16[128,2048]{1,0:T(8,128)(2,1)S(1)} custom-call(bf16[128,2048]{1,0:T(8,128)(2,1)S(1)} %all_gather.13.rows_ref, bf16[2048,1664]{1,0:T(8,128)(2,1)} %all-gather.3.cloned.1.call-done.weight_ref.last_ref, bf16[2048,1664]{1,0:T(8,128)(2,1)} %all-gather.3.cloned.1.call-done.weight_ref.last_ref, bf16[128,128]{1,0:T(8,128)(2,1)S(1)} %get-tuple-element.26.early_ref, ...), custom_call_target="tpu_custom_call" | custom-call | flops 805306368 | bytes 6291456 | tf_op jit(solution)/shard_map/feed/pallas_call | solution.py:116
  196.5 14.4 %all_to_all.10 = bf16[8,16,2048]{2,1,0:T(8,128)(2,1)S(1)} all-to-all(bf16[8,16,2048]{2,1,0:T(8,128)(2,1)S(1)} %bitcast.12), channel_id=1, replica_groups=mesh['grp'=2,'fs'=32,'tp'=8] {'tp'}, dimensions={0} | all-to-all | bytes 1048576 | tf_op jit(solution)/shard_map/all_to_all | solution.py:187
  211.2 14.1 %all_gather.15 = bf16[128,2048]{1,0:T(8,128)(2,1)S(1)} all-gather(bf16[16,2048]{1,0:T(8,128)(2,1)S(1)} %add_convert_fusion), channel_id=1, replica_groups=mesh['grp'=2,'fs'=32,'tp'=8] {'tp'}, dimensions={0}, use_global_device_ids=true | all-gather | bytes 589824 | tf_op jit(solution)/shard_map/all_gather | solution.py:275
  225.3 0.8 copy.32
  (52 shorter events, 2.3 us)
Async XLA Ops:
  6.5 185.0 %all-gather.3.cloned.1.call-start = ((), (), s32[]{:S(2)}) async-start(), calls=%async_computation.2 | async-start | bytes 7028736 | tf_op jit(solution)/shard_map/all_gather | solution.py:211
  6.6 126.1 %copy-start.9 = (f32[2048]{0:T(1024)S(1)}, f32[2048]{0:T(1024)}, u32[]{:S(2)}) copy-start(f32[2048]{0:T(1024)} %param.17) | copy-start | bytes 24580
  8.3 124.1 %collective-permute-start = (bf16[128,2048]{1,0:T(8,128)(2,1)}, bf16[128,2048]{1,0:T(8,128)(2,1)S(1)}, u32[]{:S(2)}, u32[]{:S(2)}) collective-permute-start(bf16[128,2048]{1,0:T(8,128)(2,1)} %param.16), channel_id=1, source_target_pairs={{0,256},{256,0},{1,257},{257,1},{2,258},{258,2},{3,259},{259,3},{4... | collective-permute-start | bytes 1572872 | tf_op jit(solution)/shard_map/ppermute | solution.py:225
  132.4 8.7 %copy-start.4 = (f16[2048,480]{1,0:T(8,128)(2,1)}, f16[2048,480]{1,0:T(8,128)(2,1)S(1)}, u32[]{:S(2)}) copy-start(f16[2048,480]{1,0:T(8,128)(2,1)S(1)} %all-gather.4) | copy-start | bytes 5898244
  132.6 8.2 %copy-start.5 = (bf16[128,2048]{1,0:T(8,128)(2,1)S(1)}, bf16[128,2048]{1,0:T(8,128)(2,1)}, u32[]{:S(2)}) copy-start(bf16[128,2048]{1,0:T(8,128)(2,1)} %param.16) | copy-start | bytes 1572868
  134.8 6.3 %collective-permute-start.1 = (f32[128,224]{1,0:T(8,128)}, f32[128,224]{1,0:T(8,128)}, u32[]{:S(2)}, u32[]{:S(2)}) collective-permute-start(f32[128,224]{1,0:T(8,128)} %copy.21), channel_id=1, source_target_pairs={{0,256},{256,0},{1,257},{257,1},{2,258},{258,2},{3,259},{259,3},{4... | collective-permute-start | bytes 344072 | tf_op jit(solution)/shard_map/ppermute | solution.py:225
  137.3 5.7 %copy-start = (f32[128,64]{0,1:T(8,128)S(1)}, f32[128,64]{0,1:T(8,128)}, u32[]{:S(2)}) copy-start(f32[128,64]{0,1:T(8,128)} %param.24) | copy-start | bytes 98308
  137.3 5.7 %copy-start.1 = (f32[64]{0:T(128)S(1)}, f32[64]{0:T(128)}, u32[]{:S(2)}) copy-start(f32[64]{0:T(128)} %param.23) | copy-start | bytes 772
  137.3 5.7 %copy-start.2 = (f32[128]{0:T(128)S(1)}, f32[128]{0:T(128)}, u32[]{:S(2)}) copy-start(f32[128]{0:T(128)} %param.25) | copy-start | bytes 1540
  137.3 8.5 %collective-permute-start.2 = (bf16[64,2048]{1,0:T(8,128)(2,1)S(1)}, bf16[64,2048]{1,0:T(8,128)(2,1)S(1)}, u32[]{:S(2)}, u32[]{:S(2)}) collective-permute-start(bf16[64,2048]{1,0:T(8,128)(2,1)S(1)} %bitcast.16), channel_id=1, source_target_pairs={{0,256},{256,0},{1,257},{257,1},{2,258},{258,2},{3,259},{259,3},{4... | collective-permute-start | bytes 786440 | tf_op jit(solution)/shard_map/ppermute | solution.py:225
  147.0 26.0 %all-to-all-start = ((bf16[8,16,2048]{2,1,0:T(8,128)(2,1)}), bf16[8,16,2048]{2,1,0:T(8,128)(2,1)S(1)}, u32[]{:S(2)}, u32[]{:S(2)}) async-start(bf16[8,16,2048]{2,1,0:T(8,128)(2,1)} %bitcast.6), calls=%async_computation | async-start | bytes 1048576 | tf_op jit(solution)/shard_map/all_to_all | solution.py:187
  165.1 8.0 %copy-start.3 = (bf16[2048,192]{1,0:T(8,128)(2,1)}, bf16[2048,192]{1,0:T(8,128)(2,1)S(1)}, u32[]{:S(2)}) copy-start(bf16[2048,192]{1,0:T(8,128)(2,1)S(1)} %multiply_convert_fusion) | copy-start | bytes 2359300
  165.1 8.1 %copy-start.6 = (f32[2048]{0:T(1024)S(1)}, f32[2048]{0:T(1024)}, u32[]{:S(2)}) copy-start(f32[2048]{0:T(1024)} %param.27) | copy-start | bytes 24580
  166.5 7.0 %copy-start.7 = (f32[2048]{0:T(1024)S(1)}, f32[2048]{0:T(1024)}, u32[]{:S(2)}) copy-start(f32[2048]{0:T(1024)} %param.28) | copy-start | bytes 24580
  166.5 21.5 %collective-permute-start.3 = (bf16[2048,192]{0,1:T(8,128)(2,1)}, bf16[2048,192]{0,1:T(8,128)(2,1)}, u32[]{:S(2)}, u32[]{:S(2)}) collective-permute-start(bf16[2048,192]{0,1:T(8,128)(2,1)} %copy.25), channel_id=1, source_target_pairs={{0,256},{256,0},{1,257},{257,1},{2,258},{258,2},{3,259},{259,3},{4... | collective-permute-start | bytes 2359304 | tf_op jit(solution)/shard_map/ppermute | solution.py:225
  173.4 17.1 %slice-start = ((bf16[2048,192]{1,0:T(8,128)(2,1)}), bf16[2048,128]{1,0:T(8,128)(2,1)S(1)}, s32[]{:S(2)}) async-start(bf16[2048,192]{1,0:T(8,128)(2,1)} %copy-done.3), calls=%async_computation.3 | async-start | bytes 1048576 | tf_op jit(solution)/shard_map/slice | solution.py:261
  189.3 1.7 slice-start.1
  191.5 19.6 %copy-start.8 = (f32[2048]{0:T(1024)S(1)}, f32[2048]{0:T(1024)}, u32[]{:S(2)}) copy-start(f32[2048]{0:T(1024)} %param.29) | copy-start | bytes 24580
Sparse Core Ops, SparseCore 0:
  9.4 163.4 all-gather.2

commit v4 on v3

--- a/solution.py
+++ b/solution.py
@@ -255,12 +255,11 @@
     )
     mix_part, held = lax.optimization_barrier((mix_part.astype(BF16), held))
     mixed = share_of_sum(mix_part, "tp")
-    apart_near = unscaled(held, 0, edges[2])
-    apart_far = swap(apart_near)
-    up_apart, down_apart = (
-        jnp.concatenate([w[:, lo:hi] for w in (apart_near, apart_far)], 1)
-        for lo, hi in zip(edges[:2], edges[1:3])
-    )
+    up_apart, down_apart = [], []
+    for side_by_side, lo, hi in ((up_apart, 0, edges[1]), (down_apart, edges[1], edges[2])):
+        w = unscaled(held, lo, hi)
+        side_by_side += [w, swap(w)]
+    up_apart, down_apart = (jnp.concatenate(w, 1) for w in (up_apart, down_apart))
     stream = own_tokens + root_norm(mixed, post_attention_gain)
     normed_mid = root_norm(stream, pre_feedforward_gain).astype(BF16)
     rows = lax.all_gather(normed_mid, "tp", axis=0, tiled=True)

time: 234 us -> 235 us (level)
  starting transfers between devices: 29.5 us -> 35.1 us
  local copies, waits for them, and re-layouts: 8.46 us -> 4.6 us
  blocking collectives: 158 us -> 155 us
    ppermute x4 -> x5, starting transfers between devices: 12.8 us -> 16.7 us  [local(): swap = lambda w: lax.ppermute(w, 'grp', [(i, i ^ 1) for i in range(groups)])]
    all_to_all x1, blocking collectives: 14.4 us -> 12 us  [share_of_sum(): lax.all_to_all(blocks, axis, split_axis=0, concat_axis=0, tiled=True)]
  transfers between devices with their start and end apart: 6 -> 7, of which waited for: 2 -> 2; matrix products, arithmetic and copies ran while one was open for 7% -> 6% of each run, Pallas kernels for 1% -> 1%
where the time goes in v4:
time: 235 us; the launch traced here: 234 us
  blocking collectives  155 us (66%)
  starting transfers between devices  35.1 us (15%)
  between operations  13.7 us (6%)
  Pallas kernels  9.14 us (4%)
  matrix products  7.54 us (3%)
  waiting for transfers between devices  5.77 us (2%)
  local copies, waits for them, and re-layouts  4.6 us (2%)
  other arithmetic  3.73 us (2%)
    all_gather x1, blocking collectives, local(): held = lax.all_gather(sent, 'fs', axis=0, tiled=True)  115 us
    all_to_all x1, starting transfers between devices, share_of_sum(): lax.all_to_all(blocks, axis, split_axis=0, concat_axis=0, tiled=True)  18.4 us
    ppermute x5, starting transfers between devices, local(): swap = lambda w: lax.ppermute(w, 'grp', [(i, i ^ 1) for i in range(groups)])  16.7 us
    all_gather x1, blocking collectives, local(): return lax.all_gather(out_share, 'tp', axis=0, tiled=True)  14.1 us
    all_gather x1, blocking collectives, local(): rows = lax.all_gather(normed_mid, 'tp', axis=0, tiled=True)  14 us
    all_to_all x1, blocking collectives, share_of_sum(): lax.all_to_all(blocks, axis, split_axis=0, concat_axis=0, tiled=True)  12 us
    all_to_all x1, waiting for transfers between devices, share_of_sum(): lax.all_to_all(blocks, axis, split_axis=0, concat_axis=0, tiled=True)  5.55 us
    pallas_call x1, Pallas kernels, feed(): pl.pallas_call(functools.partial(feed_body, halves), grid=(2 * halves,),...  4.98 us
  transfers between devices with their start and end apart: 7, of which 2 were waited for; matrix products, arithmetic and copies ran while one was open for 6% of the time, Pallas kernels for 1%

profile of v4, /device:TPU:33, one launch (start us, length us, event | category | flops | bytes accessed | tf_op | source)
XLA Modules:
  0.0 234.3 jit_solution(7345166991539215797)
XLA Ops:
  6.6 1.7 pack.1
  8.3 4.6 %collective-permute-start = (bf16[128,2048]{1,0:T(8,128)(2,1)}, bf16[128,2048]{1,0:T(8,128)(2,1)S(1)}, u32[]{:S(2)}, u32[]{:S(2)}) collective-permute-start(bf16[128,2048]{1,0:T(8,128)(2,1)} %param.16), channel_id=1, source_target_pairs={{0,256},{256,0},{1,257},{257,1},{2,258},{258,2},{3,259},{259,3},{4... | collective-permute-start | bytes 1572872 | tf_op jit(solution)/shard_map/ppermute | solution.py:225
  12.9 0.9 pad_maximum_fusion.1
  13.8 0.9 fusion.45
  14.7 0.7 fusion.46
  15.4 0.9 fusion.48
  16.5 114.6 %all-gather.4 = f16[2048,480]{1,0:T(8,128)(2,1)S(1)} all-gather(f16[64,480]{1,0:T(8,128)(2,1)S(1)} %multiply_convert_fusion.8), channel_id=1, replica_groups=mesh['grp'=2,'fs'=32,'tp'=8] {'fs'}, dimensions={0}, use_global_device_ids=true | all-gather | bytes 2027520 | tf_op jit(solution)/shard_map/all_gather | solution.py:227
  131.2 0.2 fusion.3
  131.4 1.3 fusion.9
  132.8 3.1 %collective-permute-start.1 = (f32[128,224]{1,0:T(8,128)S(1)}, f32[128,224]{1,0:T(8,128)}, u32[]{:S(2)}, u32[]{:S(2)}) collective-permute-start(f32[128,224]{1,0:T(8,128)S(1)} %copy.17), channel_id=1, source_target_pairs={{0,256},{256,0},{1,257},{257,1},{2,258},{258,2},{3,259},{259,3},{4... | collective-permute-start | bytes 344072 | tf_op jit(solution)/shard_map/ppermute | solution.py:225
  135.9 0.3 multiply_convert_fusion.6
  136.3 0.2 copy.20
  136.5 2.4 %collective-permute-start.2 = (bf16[64,2048]{1,0:T(8,128)(2,1)S(1)}, bf16[64,2048]{1,0:T(8,128)(2,1)S(1)}, u32[]{:S(2)}, u32[]{:S(2)}) collective-permute-start(bf16[64,2048]{1,0:T(8,128)(2,1)S(1)} %bitcast.16), channel_id=1, source_target_pairs={{0,256},{256,0},{1,257},{257,1},{2,258},{258,2},{3,259},{259,3},{4... | collective-permute-start | bytes 786440 | tf_op jit(solution)/shard_map/ppermute | solution.py:225
  139.0 0.2 fusion.6
  139.2 1.7 broadcast_select_fusion.1
  141.0 2.5 %attend.1 = bf16[128,128]{1,0:T(8,128)(2,1)S(1)} custom-call(f32[128,448]{1,0:T(8,128)S(1)} %pad_maximum_fusion.acc_ref, f32[1,64]{1,0:T(1,128)S(1)} %bitcast.14, f32[64,128]{1,0:T(8,128)S(1)} %bitcast.13, f32[1,128]{1,0:T(1,128)S(1)} %bitcast.15), custom_call_target="tpu_custom_call" | custom-call | flops 40000000 | bytes 500000 | tf_op jit(solution)/shard_map/attend/pallas_call | solution.py:68
  143.5 0.3 fusion.31
  144.0 1.1 fusion
  145.2 0.9 multiply_convert_fusion.5
  146.1 2.9 %collective-permute-start.3 = (bf16[2048,128]{1,0:T(8,128)(2,1)}, bf16[2048,128]{1,0:T(8,128)(2,1)}, u32[]{:S(2)}, u32[]{:S(2)}) collective-permute-start(bf16[2048,128]{1,0:T(8,128)(2,1)} %multiply_convert_fusion.5), channel_id=1, source_target_pairs={{0,256},{256,0},{1,257},{257,1},{2,258},{258,2},{3,259},{259,3},{4... | collective-permute-start | bytes 1572872 | tf_op jit(solution)/shard_map/ppermute | solution.py:225
  149.0 18.4 %all-to-all-start = ((bf16[8,16,2048]{2,1,0:T(8,128)(2,1)}), bf16[8,16,2048]{2,1,0:T(8,128)(2,1)S(1)}, u32[]{:S(2)}, u32[]{:S(2)}) async-start(bf16[8,16,2048]{2,1,0:T(8,128)(2,1)} %bitcast.6), calls=%async_computation | async-start | bytes 1048576 | tf_op jit(solution)/shard_map/all_to_all | solution.py:187
  167.6 3.7 %collective-permute-start.4 = (bf16[2048,64]{1,0:T(8,128)(2,1)S(1)}, bf16[2048,64]{1,0:T(8,128)(2,1)S(1)}, u32[]{:S(2)}, u32[]{:S(2)}) collective-permute-start(bf16[2048,64]{1,0:T(8,128)(2,1)S(1)} %multiply_convert_fusion.4), channel_id=1, source_target_pairs={{0,256},{256,0},{1,257},{257,1},{2,258},{258,2},{3,259},{259,3},{4... | collective-permute-start | bytes 786440 | tf_op jit(solution)/shard_map/ppermute | solution.py:225
  171.2 5.6 %all-to-all-done = bf16[8,16,2048]{2,1,0:T(8,128)(2,1)S(1)} async-done(((bf16[8,16,2048]{2,1,0:T(8,128)(2,1)}), bf16[8,16,2048]{2,1,0:T(8,128)(2,1)S(1)}, u32[]{:S(2)}, u32[]{:S(2)}) %all-to-all-start) | async-done | bytes 524320 | tf_op jit(solution)/shard_map/all_to_all | solution.py:187
  177.0 0.2 multiply_reduce_fusion.1
  177.3 14.0 %all_gather.13.rows_ref = bf16[128,2048]{1,0:T(8,128)(2,1)S(1)} all-gather(bf16[16,2048]{1,0:T(8,128)(2,1)S(1)} %multiply_convert_fusion.7), channel_id=1, replica_groups=mesh['grp'=2,'fs'=32,'tp'=8] {'tp'}, dimensions={0}, use_global_device_ids=true | all-gather | bytes 589824 | tf_op jit(solution)/shard_map/all_gather | solution.py:265
  191.3 1.5 fusion.2
  193.0 0.8 copy-done.4
  193.7 1.5 fusion.20.part_ref
  195.3 5.0 %feed.1 = bf16[128,2048]{1,0:T(8,128)(2,1)S(1)} custom-call(bf16[128,2048]{1,0:T(8,128)(2,1)S(1)} %all_gather.13.rows_ref, bf16[2048,1664]{1,0:T(8,128)(2,1)} %all-gather.3.cloned.1.call-done.weight_ref.last_ref, bf16[2048,1664]{1,0:T(8,128)(2,1)} %all-gather.3.cloned.1.call-done.weight_ref.last_ref, bf16[128,128]{1,0:T(8,128)(2,1)S(1)} %get-tuple-element.26.early_ref, ...), custom_call_target="tpu_custom_call" | custom-call | flops 805306368 | bytes 6291456 | tf_op jit(solution)/shard_map/feed/pallas_call | solution.py:116
  200.3 12.0 %all_to_all.10 = bf16[8,16,2048]{2,1,0:T(8,128)(2,1)S(1)} all-to-all(bf16[8,16,2048]{2,1,0:T(8,128)(2,1)S(1)} %bitcast.12), channel_id=1, replica_groups=mesh['grp'=2,'fs'=32,'tp'=8] {'tp'}, dimensions={0} | all-to-all | bytes 1048576 | tf_op jit(solution)/shard_map/all_to_all | solution.py:187
  212.6 14.1 %all_gather.15 = bf16[128,2048]{1,0:T(8,128)(2,1)S(1)} all-gather(bf16[16,2048]{1,0:T(8,128)(2,1)S(1)} %add_convert_fusion), channel_id=1, replica_groups=mesh['grp'=2,'fs'=32,'tp'=8] {'tp'}, dimensions={0}, use_global_device_ids=true | all-gather | bytes 589824 | tf_op jit(solution)/shard_map/all_gather | solution.py:274
  226.7 0.8 copy.23
  (44 shorter events, 1.6 us)
Async XLA Ops:
  6.5 188.7 %all-gather.3.cloned.1.call-start = ((), (), s32[]{:S(2)}) async-start(), calls=%async_computation.2 | async-start | bytes 7028736 | tf_op jit(solution)/shard_map/all_gather | solution.py:211
  6.6 124.8 %copy-start.8 = (f32[2048]{0:T(1024)S(1)}, f32[2048]{0:T(1024)}, u32[]{:S(2)}) copy-start(f32[2048]{0:T(1024)} %param.17) | copy-start | bytes 24580
  8.3 122.9 %collective-permute-start = (bf16[128,2048]{1,0:T(8,128)(2,1)}, bf16[128,2048]{1,0:T(8,128)(2,1)S(1)}, u32[]{:S(2)}, u32[]{:S(2)}) collective-permute-start(bf16[128,2048]{1,0:T(8,128)(2,1)} %param.16), channel_id=1, source_target_pairs={{0,256},{256,0},{1,257},{257,1},{2,258},{258,2},{3,259},{259,3},{4... | collective-permute-start | bytes 1572872 | tf_op jit(solution)/shard_map/ppermute | solution.py:225
  131.4 7.5 %copy-start.3 = (bf16[128,2048]{1,0:T(8,128)(2,1)S(1)}, bf16[128,2048]{1,0:T(8,128)(2,1)}, u32[]{:S(2)}) copy-start(bf16[128,2048]{1,0:T(8,128)(2,1)} %param.16) | copy-start | bytes 1572868
  132.8 6.3 %collective-permute-start.1 = (f32[128,224]{1,0:T(8,128)S(1)}, f32[128,224]{1,0:T(8,128)}, u32[]{:S(2)}, u32[]{:S(2)}) collective-permute-start(f32[128,224]{1,0:T(8,128)S(1)} %copy.17), channel_id=1, source_target_pairs={{0,256},{256,0},{1,257},{257,1},{2,258},{258,2},{3,259},{259,3},{4... | collective-permute-start | bytes 344072 | tf_op jit(solution)/shard_map/ppermute | solution.py:225
  136.5 4.5 %copy-start = (f32[128,64]{0,1:T(8,128)S(1)}, f32[128,64]{0,1:T(8,128)}, u32[]{:S(2)}) copy-start(f32[128,64]{0,1:T(8,128)} %param.24) | copy-start | bytes 98308
  136.5 4.5 %copy-start.1 = (f32[64]{0:T(128)S(1)}, f32[64]{0:T(128)}, u32[]{:S(2)}) copy-start(f32[64]{0:T(128)} %param.23) | copy-start | bytes 772
  136.5 4.5 %copy-start.2 = (f32[128]{0:T(128)S(1)}, f32[128]{0:T(128)}, u32[]{:S(2)}) copy-start(f32[128]{0:T(128)} %param.25) | copy-start | bytes 1540
  136.5 7.5 %collective-permute-start.2 = (bf16[64,2048]{1,0:T(8,128)(2,1)S(1)}, bf16[64,2048]{1,0:T(8,128)(2,1)S(1)}, u32[]{:S(2)}, u32[]{:S(2)}) collective-permute-start(bf16[64,2048]{1,0:T(8,128)(2,1)S(1)} %bitcast.16), channel_id=1, source_target_pairs={{0,256},{256,0},{1,257},{257,1},{2,258},{258,2},{3,259},{259,3},{4... | collective-permute-start | bytes 786440 | tf_op jit(solution)/shard_map/ppermute | solution.py:225
  145.1 31.8 %copy-start.5 = (f32[2048]{0:T(1024)S(1)}, f32[2048]{0:T(1024)}, u32[]{:S(2)}) copy-start(f32[2048]{0:T(1024)} %param.27) | copy-start | bytes 24580
  145.1 32.1 %copy-start.6 = (f32[2048]{0:T(1024)S(1)}, f32[2048]{0:T(1024)}, u32[]{:S(2)}) copy-start(f32[2048]{0:T(1024)} %param.28) | copy-start | bytes 24580
  146.1 45.2 %collective-permute-start.3 = (bf16[2048,128]{1,0:T(8,128)(2,1)}, bf16[2048,128]{1,0:T(8,128)(2,1)}, u32[]{:S(2)}, u32[]{:S(2)}) collective-permute-start(bf16[2048,128]{1,0:T(8,128)(2,1)} %multiply_convert_fusion.5), channel_id=1, source_target_pairs={{0,256},{256,0},{1,257},{257,1},{2,258},{258,2},{3,259},{259,3},{4... | collective-permute-start | bytes 1572872 | tf_op jit(solution)/shard_map/ppermute | solution.py:225
  149.0 27.8 %all-to-all-start = ((bf16[8,16,2048]{2,1,0:T(8,128)(2,1)}), bf16[8,16,2048]{2,1,0:T(8,128)(2,1)S(1)}, u32[]{:S(2)}, u32[]{:S(2)}) async-start(bf16[8,16,2048]{2,1,0:T(8,128)(2,1)} %bitcast.6), calls=%async_computation | async-start | bytes 1048576 | tf_op jit(solution)/shard_map/all_to_all | solution.py:187
  167.6 25.4 %collective-permute-start.4 = (bf16[2048,64]{1,0:T(8,128)(2,1)S(1)}, bf16[2048,64]{1,0:T(8,128)(2,1)S(1)}, u32[]{:S(2)}, u32[]{:S(2)}) collective-permute-start(bf16[2048,64]{1,0:T(8,128)(2,1)S(1)} %multiply_convert_fusion.4), channel_id=1, source_target_pairs={{0,256},{256,0},{1,257},{257,1},{2,258},{258,2},{3,259},{259,3},{4... | collective-permute-start | bytes 786440 | tf_op jit(solution)/shard_map/ppermute | solution.py:225
  192.9 0.8 copy-start.4
  195.3 17.2 %copy-start.7 = (f32[2048]{0:T(1024)S(1)}, f32[2048]{0:T(1024)}, u32[]{:S(2)}) copy-start(f32[2048]{0:T(1024)} %param.29) | copy-start | bytes 24580
Sparse Core Ops, SparseCore 0:
  9.4 163.5 all-gather.2
